TPU v7x, 32 devices: a whole 2x2x4 slice. The times are simulated.
32 devices in a mesh: sp: 8 (over z, x), tp: 4 (over y, core).
Axes of the slice: x: 2, y: 2, z: 4, core: 2. Of those that a mesh axis runs over, the one named last changes fastest.
Arguments:
- tokens_in: bfloat16 [4096, 4096], P(('sp', 'tp')), may hold values from -64 to 64
- w_query: bfloat16 [4096, 2048], P(None, 'tp'), may hold values from -0.09375 to 0.09375
- w_key: bfloat16 [4096, 2048], P(None, 'tp'), may hold values from -0.09375 to 0.09375
- w_value: bfloat16 [4096, 2048], P(None, 'tp'), may hold values from -0.09375 to 0.09375
- w_out: bfloat16 [2048, 4096], P('tp'), may hold values from -1 to 1
Outputs:
- mixed: bfloat16 [4096, 4096], P(('sp', 'tp'))
- log_weight: float32 [32, 4096], P('tp', 'sp')
All inputs are finite; a program needn't handle non-finite values.
Results may differ from a plain program's by a relative error of at most 0.019.
Values may be sent and summed in bfloat16 or wider, within the bound.
A program may use at most 128 MiB of HBM per device.

v0:
```python
import functools

import jax
import jax.numpy as jnp
import numpy as np
from jax import lax
from jax.experimental import pallas as pl
from jax.experimental.pallas import tpu as pltpu
from jax.sharding import PartitionSpec as P

HEAD_DIM = 64
SIDE_SPAN = 64
MIDDLE_DILATION = 8
WIDEST_DILATION = 64


ROTARY_BASE = 500000.0
NEGATIVE = -1e30


def shifted(block, axis, distance):
    devices = range(lax.axis_size(axis))
    route = [(i - distance, i) for i in devices if i - distance in devices]
    return lax.ppermute(block, axis, route)


def rotate(block, positions):
    half_size = block.shape[-1] // 2
    freq = 1.0 / ROTARY_BASE ** (jnp.arange(half_size, dtype=jnp.float32) / half_size)
    angle = positions[:, None] * freq[None, :]
    cosine = jnp.cos(angle)[:, None, :]
    sine = jnp.sin(angle)[:, None, :]
    front = block[..., :half_size]
    back = block[..., half_size:]
    return jnp.concatenate([front * cosine - back * sine, back * cosine + front * sine], axis=-1)


def pattern_attend(query, keys, values, lead_rows, dilation_step, low_row, high_row):
    rows_total, head_count, head_size = query.shape
    class_len = rows_total // dilation_step
    first_class = lead_rows // dilation_step - SIDE_SPAN
    class_q = query.reshape(class_len, dilation_step, head_count, head_size)
    class_k = keys.reshape(keys.shape[0] // dilation_step, dilation_step, head_count, head_size)
    class_v = values.reshape(values.shape[0] // dilation_step, dilation_step, head_count, head_size)
    sub_k = class_k[first_class : first_class + class_len + 2 * SIDE_SPAN]
    sub_v = class_v[first_class : first_class + class_len + 2 * SIDE_SPAN]
    if class_len <= SIDE_SPAN:
        block_len = class_len
        block_count = 1
        win_k = sub_k[None]
        win_v = sub_v[None]
        blocks_q = class_q[None]
    else:
        block_len = SIDE_SPAN
        block_count = class_len // SIDE_SPAN
        part_k = sub_k.reshape(block_count + 2, SIDE_SPAN, dilation_step, head_count, head_size)
        part_v = sub_v.reshape(block_count + 2, SIDE_SPAN, dilation_step, head_count, head_size)
        win_k = jnp.concatenate([part_k[:-2], part_k[1:-1], part_k[2:]], axis=1)
        win_v = jnp.concatenate([part_v[:-2], part_v[1:-1], part_v[2:]], axis=1)
        blocks_q = class_q.reshape(block_count, SIDE_SPAN, dilation_step, head_count, head_size)
    width = block_len + 2 * SIDE_SPAN
    scores = jnp.einsum("nasht,nksht->nshak", blocks_q, win_k, preferred_element_type=jnp.float32)
    scores = scores * head_size ** (-0.5)
    q_index = jnp.arange(block_len, dtype=jnp.int32)
    k_index = jnp.arange(width, dtype=jnp.int32)
    b_index = jnp.arange(block_count, dtype=jnp.int32)
    s_index = jnp.arange(dilation_step, dtype=jnp.int32)
    in_band = jnp.abs(k_index[None, :] - SIDE_SPAN - q_index[:, None]) <= SIDE_SPAN
    key_position = (
        (first_class + b_index[:, None] * block_len + k_index[None, :]) * dilation_step
    )[:, None, :] + s_index[None, :, None]
    is_valid = (key_position >= low_row) & (key_position < high_row)
    keep_mask = in_band[None, None, None] & is_valid[:, :, None, None, :]
    scores = jnp.where(keep_mask, scores, NEGATIVE)
    maxima = jnp.max(scores, axis=-1, keepdims=True)
    expo = jnp.exp(scores - maxima)
    totals = jnp.sum(expo, axis=-1)
    numerator = jnp.einsum(
        "nshak,nksht->nasht", expo.astype(jnp.bfloat16), win_v, preferred_element_type=jnp.float32
    )
    totals_t = jnp.transpose(totals, (0, 3, 1, 2))
    result = (
        (numerator / totals_t[..., None])
        .astype(jnp.bfloat16)
        .reshape(rows_total, head_count, head_size)
    )
    log_sum = jnp.transpose(maxima[..., 0] + jnp.log(totals), (0, 3, 1, 2)).reshape(
        rows_total, head_count
    )
    return (result, log_sum)


def combine(results):
    sums = jnp.stack([item[1] for item in results], axis=0)
    peak = jnp.max(sums, axis=0)
    share = jnp.exp(sums - peak[None])
    weight_sum = share[0] + share[1] + share[2]
    accum = share[0][..., None] * results[0][0].astype(jnp.float32)
    accum = accum + share[1][..., None] * results[1][0].astype(jnp.float32)
    accum = accum + share[2][..., None] * results[2][0].astype(jnp.float32)
    attended = (accum / weight_sum[..., None]).astype(jnp.bfloat16)
    return (attended, peak + jnp.log(weight_sum))


def per_device(tokens_in, w_query, w_key, w_value, w_out):
    col_count = w_query.shape[1]
    head_count = col_count // HEAD_DIM
    piece = lax.all_gather(tokens_in, "tp", axis=0, tiled=True)
    projected = jnp.concatenate(
        [
            jnp.dot(piece, w_query, preferred_element_type=jnp.float32),
            jnp.dot(piece, w_key, preferred_element_type=jnp.float32),
            jnp.dot(piece, w_value, preferred_element_type=jnp.float32),
        ],
        axis=1,
    )
    rows_total = projected.shape[0]
    sp_size = lax.axis_size("sp")
    sp_place = lax.axis_index("sp")
    positions = (sp_place * rows_total + jnp.arange(rows_total, dtype=jnp.int32)).astype(
        jnp.float32
    )
    shape3 = (rows_total, head_count, HEAD_DIM)
    query = rotate(projected[:, :col_count].reshape(shape3), positions).astype(jnp.bfloat16)
    keys = rotate(projected[:, col_count : 2 * col_count].reshape(shape3), positions).astype(
        jnp.bfloat16
    )
    values = projected[:, 2 * col_count :].astype(jnp.bfloat16).reshape(shape3)
    per_device_span = -(-(SIDE_SPAN * MIDDLE_DILATION) // rows_total)
    earlier_k = []
    earlier_v = []
    before_k, before_v = shifted((keys, values), "sp", 1)
    after_k, after_v = shifted((keys, values), "sp", -1)
    earlier_k.insert(0, before_k)
    earlier_v.insert(0, before_v)
    later_k = [after_k]
    later_v = [after_v]
    key_buf = jnp.concatenate(earlier_k + [keys] + later_k, axis=0)
    value_buf = jnp.concatenate(earlier_v + [values] + later_v, axis=0)
    lead_rows = per_device_span * rows_total
    low_row = lead_rows - sp_place * rows_total
    key_buf, value_buf, lead_rows, low_row, high_row = (
        key_buf,
        value_buf,
        lead_rows,
        low_row,
        low_row + sp_size * rows_total,
    )
    results = [
        pattern_attend(query, key_buf, value_buf, lead_rows, dilation_step, low_row, high_row)
        for dilation_step in (1, MIDDLE_DILATION)
    ]
    class_stride = WIDEST_DILATION // sp_size
    border_extent = SIDE_SPAN * class_stride
    class_shape = (rows_total // sp_size, sp_size, head_count, HEAD_DIM)
    parts = (
        lax.all_to_all(query.reshape(class_shape), "sp", split_axis=1, concat_axis=0, tiled=True),
        lax.all_to_all(keys.reshape(class_shape), "sp", split_axis=1, concat_axis=0, tiled=True),
        lax.all_to_all(values.reshape(class_shape), "sp", split_axis=1, concat_axis=0, tiled=True),
    )
    item_heads = parts[0].shape[2]
    flat = [item.reshape(rows_total, item_heads, HEAD_DIM) for item in parts]
    pad_k = jnp.pad(flat[1], ((border_extent, border_extent), (0, 0), (0, 0)))
    pad_v = jnp.pad(flat[2], ((border_extent, border_extent), (0, 0), (0, 0)))
    result, log_sum = pattern_attend(
        flat[0],
        pad_k,
        pad_v,
        border_extent,
        class_stride,
        border_extent,
        border_extent + rows_total,
    )
    result_back = lax.all_to_all(
        result.reshape(rows_total, 1, item_heads, HEAD_DIM),
        "sp",
        split_axis=0,
        concat_axis=1,
        tiled=True,
    )
    sum_back = lax.all_to_all(
        log_sum.reshape(rows_total, 1, item_heads), "sp", split_axis=0, concat_axis=1, tiled=True
    )
    results.append((result_back.reshape(shape3), sum_back.reshape(rows_total, head_count)))
    attended, log_weight = combine(results)
    flat_out = attended.reshape(rows_total, col_count)
    mixed = lax.psum_scatter(
        jnp.dot(flat_out, w_out, preferred_element_type=jnp.float32).astype(jnp.bfloat16),
        "tp",
        scatter_dimension=0,
        tiled=True,
    )
    return (mixed, jnp.transpose(log_weight, (1, 0)))


MESH_ID = pl.DeviceIdType.MESH
PAIR = 2 * HEAD_DIM
ROW_BLOCK = 128
SPLITS = 2
OUT_SPLITS = 4


def class_kernel(
    sp_size, tp_size, col_count,
    x_hbm, wq_hbm, wk_hbm, wv_hbm, wo_hbm, base_ref, local_cos, local_sin,
    out_ref, logw_ref,
    x_all, w_all, wo, cos_t, sin_t, q_c, kv_ext, pf, cls_send, cls_recv,
    bias_near, bias_class, o_near, lse_near, cls_o, cls_lse, lse_out, ret, ret_lse, ret_f, lse_f, att,
    part_out, part_in, cross_out, cross_in, keep_b, keep_d,
    load_sem, own_send, own_recv, far_send, far_recv, fwd_send, fwd_recv,
    a2a_send, a2a_recv, halo_send, halo_recv, back_send, back_recv, lback_send, lback_recv,
    ex_send, ex_recv, cr_send, cr_recv,
):
    sp = lax.axis_index("sp")
    tp = lax.axis_index("tp")
    chips = tp_size // 2
    chip = tp // 2
    core = tp % 2
    partner = chip * 2 + (1 - core)
    shard = x_hbm.shape[0]
    rows = shard * tp_size
    piece = shard // SPLITS
    group_count = col_count // PAIR
    head_count = col_count // HEAD_DIM
    cls_rows = rows // sp_size
    chip_rows = 2 * shard
    chip_cls = chip_rows // sp_size
    f32, bf16 = jnp.float32, jnp.bfloat16

    offsets = sorted(range(1, sp_size), key=lambda off: (abs(off - sp_size // 2), off))

    def chip_at(d):
        return (chip + d) % chips

    loads = [pltpu.make_async_copy(x_hbm, x_all.at[tp], load_sem.at[0])]
    for n, w in enumerate((wq_hbm, wk_hbm, wv_hbm)):
        loads.append(pltpu.make_async_copy(w, w_all.at[n], load_sem.at[1 + n]))
    loads.append(pltpu.make_async_copy(wo_hbm, wo, load_sem.at[4]))
    for item in loads[:4]:
        item.start()

    barrier = pltpu.get_barrier_semaphore()
    pl.semaphore_signal(barrier, inc=1, device_id={"tp": partner}, device_id_type=MESH_ID)
    for d in range(1, chips):
        pl.semaphore_signal(
            barrier, inc=1, device_id={"tp": chip_at(d) * 2 + core}, device_id_type=MESH_ID
        )
    for off in offsets:
        pl.semaphore_signal(
            barrier, inc=1, device_id={"sp": (sp + off) % sp_size}, device_id_type=MESH_ID
        )
    pl.semaphore_wait(barrier, 1 + (chips - 1) + (sp_size - 1))

    def remote(src, dst, send, recv, **where):
        return pltpu.make_async_remote_copy(
            src_ref=src, dst_ref=dst, send_sem=send, recv_sem=recv,
            device_id=where, device_id_type=MESH_ID,
        )

    waits = []
    far = {}
    for k in range(SPLITS):
        for d in range(1, chips):
            span = pl.ds(k * piece, piece)
            far[d, k] = remote(
                x_hbm.at[span], x_all.at[tp, span], far_send.at[d, k], far_recv.at[d, k],
                tp=chip_at(d) * 2 + core,
            )
            far[d, k].start()
            waits.append(far[d, k])
    own = remote(x_hbm, x_all.at[tp], own_send.at[0], own_recv.at[0], tp=partner)
    own.start()
    waits.append(own)
    loads[4].start()

    base_cos = base_ref[0, pl.ds(sp, 1), :]
    base_sin = base_ref[1, pl.ds(sp, 1), :]
    lane = lax.broadcasted_iota(jnp.int32, (1, PAIR), 1)
    front = lane % HEAD_DIM < HEAD_DIM // 2
    first_head = lane < HEAD_DIM
    sign = jnp.where(front, -1.0, 1.0).astype(f32)
    for r0 in range(0, rows, ROW_BLOCK):
        lc = local_cos[r0 : r0 + ROW_BLOCK]
        ls = local_sin[r0 : r0 + ROW_BLOCK]
        cos_t[r0 : r0 + ROW_BLOCK] = lc * base_cos - ls * base_sin
        sin_t[r0 : r0 + ROW_BLOCK] = (ls * base_cos + lc * base_sin) * sign
    window = ROW_BLOCK + 2 * SIDE_SPAN
    near_i = lax.broadcasted_iota(jnp.int32, (ROW_BLOCK, window), 0)
    near_j = lax.broadcasted_iota(jnp.int32, (ROW_BLOCK, window), 1)
    near_band = jnp.abs(near_j - SIDE_SPAN - near_i) <= SIDE_SPAN
    mid_step = MIDDLE_DILATION // sp_size
    wide_step = WIDEST_DILATION // sp_size
    for r0 in range(0, rows, ROW_BLOCK):
        key_pos = sp * rows + r0 + near_j - SIDE_SPAN
        good = near_band & (key_pos >= 0) & (key_pos < sp_size * rows)
        bias_near[r0 : r0 + ROW_BLOCK] = jnp.where(good, 0.0, NEGATIVE)
        gap = jnp.abs(
            lax.broadcasted_iota(jnp.int32, (ROW_BLOCK, rows), 0)
            + r0
            - lax.broadcasted_iota(jnp.int32, (ROW_BLOCK, rows), 1)
        )
        mid = (gap % mid_step == 0) & (gap <= SIDE_SPAN * mid_step)
        wide = (gap % wide_step == 0) & (gap <= SIDE_SPAN * wide_step)
        bias_class[r0 : r0 + ROW_BLOCK] = jnp.where(
            mid & wide, float(np.log(2.0)), jnp.where(mid | wide, 0.0, NEGATIVE)
        )

    def turn(x, cos, sin):
        swapped = jnp.where(
            front, pltpu.roll(x, PAIR - HEAD_DIM // 2, 1), pltpu.roll(x, HEAD_DIM // 2, 1)
        )
        return x * cos + swapped * sin

    def project(spans):
        for n in range(3):
            if len(spans) == 1:
                left = x_all[spans[0][0], pl.ds(spans[0][1], spans[0][2])]
            else:
                left = jnp.concatenate([x_all[s, pl.ds(a, c)] for s, a, c in spans], axis=0)
            full = jnp.dot(left, w_all[n], preferred_element_type=f32)
            at = 0
            for s, a, c in spans:
                r0 = pl.multiple_of(s * shard + a, c)
                cos = cos_t[pl.ds(r0, c)]
                sin = sin_t[pl.ds(r0, c)]
                for g in range(group_count):
                    part = full[at : at + c, g * PAIR : (g + 1) * PAIR]
                    if n < 2:
                        part = turn(part, cos, sin)
                    pf[n * group_count + g, pl.ds(r0, c), :] = part
                    low = part.astype(bf16)
                    if n == 0:
                        q_c[pl.ds(r0, c), g * PAIR : (g + 1) * PAIR] = low
                    else:
                        kv_ext[
                            pl.ds(r0 + SIDE_SPAN, c),
                            (n - 1) * col_count + g * PAIR : (n - 1) * col_count + (g + 1) * PAIR,
                        ] = low
                at += c

    a2a = {}

    def scatter(d):
        which = chip_at(d)
        base = pl.multiple_of(which * chip_cls, chip_cls)

        def one(r, carry):
            for g in range(3 * group_count):
                cls_send[r, pl.ds(base, chip_cls), g * PAIR : (g + 1) * PAIR] = pf[
                    g, pl.ds(which * chip_rows + r, chip_cls, stride=sp_size), :
                ].astype(bf16)
            return carry

        lax.fori_loop(0, sp_size, one, 0)
        mine = pl.ds(pl.multiple_of(sp * cls_rows + base, chip_cls), chip_cls)
        for off in offsets:
            dest = (sp + off) % sp_size
            a2a[d, off] = remote(
                cls_send.at[dest, pl.ds(base, chip_cls)], cls_recv.at[mine],
                a2a_send.at[d, off], a2a_recv.at[d, off], sp=dest,
            )
            a2a[d, off].start()
        cls_recv[mine, :] = cls_send[sp, pl.ds(base, chip_cls), :]

    for item in loads[:4]:
        item.wait()
    project([(tp, 0, shard)])
    own.wait_recv()
    project([(partner, 0, shard)])
    scatter(0)
    fwd = {}
    for d in range(1, chips):
        src = chip_at(d) * 2 + core
        other = chip_at(d) * 2 + 1 - core
        e = chips - d
        for k in range(SPLITS):
            span = pl.ds(k * piece, piece)
            far[e, k].wait_recv()
            fwd[d, k] = remote(
                x_all.at[src, span], x_all.at[src, span], fwd_send.at[d, k], fwd_recv.at[d, k],
                tp=partner,
            )
            fwd[d, k].start()
            waits.append(fwd[d, k])
            fwd[d, k].wait_recv()
            project([(src, k * piece, piece), (other, k * piece, piece)])
        if d == chips - 1:
            halo = [
                remote(
                    kv_ext.at[pl.ds(rows, SIDE_SPAN)], kv_ext.at[pl.ds(0, SIDE_SPAN)],
                    halo_send.at[0], halo_recv.at[0], sp=(sp + 1) % sp_size,
                ),
                remote(
                    kv_ext.at[pl.ds(SIDE_SPAN, SIDE_SPAN)],
                    kv_ext.at[pl.ds(rows + SIDE_SPAN, SIDE_SPAN)],
                    halo_send.at[1], halo_recv.at[1], sp=(sp + sp_size - 1) % sp_size,
                ),
            ]
            for item in halo:
                item.start()
        scatter(d)

    lane_wide = lax.broadcasted_iota(jnp.int32, (ROW_BLOCK, PAIR), 1)
    scale = HEAD_DIM ** (-0.5)

    def attend(query, keys, values, bias):
        outs, sums = [], []
        for half in range(2):
            pick = first_head if half == 0 else jnp.logical_not(first_head)
            q = jnp.where(pick, query.astype(f32) * scale, 0.0).astype(bf16)
            s = lax.dot_general(q, keys, (((1,), (1,)), ((), ())), preferred_element_type=f32)
            s = s + bias
            top = jnp.max(s, axis=1, keepdims=True)
            e = jnp.exp(s - top)
            total = jnp.sum(e, axis=1, keepdims=True)
            o = jnp.dot(e.astype(bf16), values, preferred_element_type=f32)
            outs.append(o / total)
            sums.append(top + jnp.log(total))
        return jnp.where(first_head, outs[0], outs[1]), sums

    for item in halo:
        item.wait_recv()

    def near_pair(g, carry):
        c0 = pl.multiple_of(g * PAIR, PAIR)
        for r0 in range(0, rows, ROW_BLOCK):
            span = slice(r0, r0 + ROW_BLOCK)
            o, sums = attend(
                q_c[span, pl.ds(c0, PAIR)],
                kv_ext[r0 : r0 + window, pl.ds(c0, PAIR)],
                kv_ext[r0 : r0 + window, pl.ds(c0 + col_count, PAIR)],
                bias_near[span],
            )
            o_near[g, span, :] = o
            kept = lse_near[span]
            kept = jnp.where(lane_wide == 2 * g, sums[0], kept)
            lse_near[span] = jnp.where(lane_wide == 2 * g + 1, sums[1], kept)
        return carry

    lse_near[...] = jnp.zeros_like(lse_near)
    cls_lse[...] = jnp.zeros_like(cls_lse)
    lax.fori_loop(0, group_count, near_pair, 0)

    for d in range(chips):
        for off in offsets:
            a2a[d, off].wait_recv()

    my_rows = pl.ds(pl.multiple_of(sp * cls_rows, cls_rows), cls_rows)

    def back(g, off):
        dest = (sp + off) % sp_size
        lanes = pl.ds(pl.multiple_of(g * PAIR, PAIR), PAIR)
        return remote(
            cls_o.at[pl.ds(pl.multiple_of(dest * cls_rows, cls_rows), cls_rows), lanes],
            ret.at[my_rows, lanes], back_send.at[g, off], back_recv.at[g, off], sp=dest,
        )

    def class_pair(g, carry):
        c0 = pl.multiple_of(g * PAIR, PAIR)
        keys = cls_recv[:, pl.ds(c0 + col_count, PAIR)]
        values = cls_recv[:, pl.ds(c0 + 2 * col_count, PAIR)]
        for r0 in range(0, rows, ROW_BLOCK):
            span = slice(r0, r0 + ROW_BLOCK)
            o, sums = attend(cls_recv[span, pl.ds(c0, PAIR)], keys, values, bias_class[span])
            cls_o[span, pl.ds(c0, PAIR)] = o.astype(bf16)
            kept = cls_lse[span]
            kept = jnp.where(lane_wide == 2 * g, sums[0], kept)
            cls_lse[span] = jnp.where(lane_wide == 2 * g + 1, sums[1], kept)
        for off in offsets:
            back(g, off).start()
        ret[my_rows, pl.ds(c0, PAIR)] = cls_o[my_rows, pl.ds(c0, PAIR)]
        return carry

    lax.fori_loop(0, group_count, class_pair, 0)
    for at in range(rows // PAIR):
        flat = jnp.transpose(cls_lse[at * PAIR : (at + 1) * PAIR])[:head_count]
        lse_out[at] = flat
    lback = []
    for off in offsets:
        dest = (sp + off) % sp_size
        item = remote(
            lse_out.at[dest * cls_rows // PAIR], ret_lse.at[sp],
            lback_send.at[off], lback_recv.at[off], sp=dest,
        )
        item.start()
        lback.append(item)
    ret_lse[sp] = lse_out[sp * cls_rows // PAIR]
    loads[4].wait()
    for item in lback:
        item.wait_recv()
    part_of = (sp * cls_rows % PAIR) // cls_rows
    for r in range(sp_size):
        tall = jnp.concatenate(
            [ret_lse[r], jnp.zeros((PAIR - head_count, PAIR), f32)], axis=0
        )
        tall = jnp.transpose(tall)
        mine = tall[:cls_rows]
        for q in range(1, PAIR // cls_rows):
            mine = jnp.where(part_of == q, tall[q * cls_rows : (q + 1) * cls_rows], mine)
        lse_f[pl.ds(r, cls_rows, stride=sp_size), :] = mine
    for g in range(group_count):
        for off in offsets:
            back(g, off).wait_recv()
        for r in range(sp_size):
            ret_f[g, pl.ds(r, cls_rows, stride=sp_size), :] = ret[
                r * cls_rows : (r + 1) * cls_rows, g * PAIR : (g + 1) * PAIR
            ].astype(f32)

    for r0 in range(0, rows, ROW_BLOCK):
        span = slice(r0, r0 + ROW_BLOCK)
        la = lse_near[span]
        lb = lse_f[span]
        peak = jnp.maximum(la, lb)
        ea = jnp.exp(la - peak)
        eb = jnp.exp(lb - peak)
        total = ea + eb
        logw = peak + jnp.log(total)
        logw_ref[:, span] = jnp.transpose(logw)[:head_count]
        ea = ea / total
        eb = eb / total
        for g in range(group_count):
            wa = jnp.where(first_head, ea[:, 2 * g : 2 * g + 1], ea[:, 2 * g + 1 : 2 * g + 2])
            wb = jnp.where(first_head, eb[:, 2 * g : 2 * g + 1], eb[:, 2 * g + 1 : 2 * g + 2])
            mixed = wa * o_near[g, span, :] + wb * ret_f[g, span, :]
            att[span, g * PAIR : (g + 1) * PAIR] = mixed.astype(bf16)

    width = wo.shape[1] // OUT_SPLITS

    def product(place, n):
        left = att[pl.ds(pl.multiple_of(place * shard, shard), shard), :]
        return jnp.dot(left, wo[:, n * width : (n + 1) * width], preferred_element_type=f32).astype(bf16)

    exch, cross = {}, {}
    steps = [(d, n) for d in range(1, chips) for n in range(OUT_SPLITS)]

    def relay(d, n):
        exch[d, n].wait_recv()
        cross_out[d, n] = (keep_b[d, n].astype(f32) + part_in[d, n].astype(f32)).astype(bf16)
        cross[d, n] = remote(
            cross_out.at[d, n], cross_in.at[d, n], cr_send.at[d, n], cr_recv.at[d, n],
            tp=chip_at(d) * 2 + core,
        )
        cross[d, n].start()
        waits.append(cross[d, n])

    def exchange(d, n):
        part_out[d, n] = product(chip_at(d) * 2 + 1 - core, n)
        exch[d, n] = remote(
            part_out.at[d, n], part_in.at[d, n], ex_send.at[d, n], ex_recv.at[d, n], tp=partner
        )
        exch[d, n].start()
        waits.append(exch[d, n])

    for at, (d, n) in enumerate(steps):
        exchange(d, n)
        keep_b[d, n] = product(chip_at(d) * 2 + core, n)
        if at:
            relay(*steps[at - 1])
    relay(*steps[-1])
    for n in range(OUT_SPLITS):
        exchange(0, n)
        keep_d[n] = product(tp, n)
    for n in range(OUT_SPLITS):
        exch[0, n].wait_recv()
        total = keep_d[n].astype(f32) + part_in[0, n].astype(f32)
        for d in range(1, chips):
            cross[d, n].wait_recv()
            total = total + cross_in[d, n].astype(f32)
        out_ref[:, n * width : (n + 1) * width] = total.astype(bf16)

    for item in waits:
        item.wait_send()
    for item in a2a.values():
        item.wait_send()
    for item in halo:
        item.wait_send()
    for item in lback:
        item.wait_send()
    for g in range(group_count):
        for off in offsets:
            back(g, off).wait_send()


def fused(sp_size, tp_size, tokens_in, w_query, w_key, w_value, w_out):
    shard, depth = tokens_in.shape
    col_count = w_query.shape[1]
    rows = shard * tp_size
    chips = tp_size // 2
    groups = col_count // PAIR
    cls_rows = rows // sp_size
    wide = w_out.shape[1]
    width = wide // OUT_SPLITS
    half = HEAD_DIM // 2
    freq = 1.0 / ROTARY_BASE ** (np.arange(half) / half)
    freq = np.tile(freq, PAIR // half)
    local = np.arange(rows)[:, None] * freq[None, :]
    start = (np.arange(sp_size) * rows)[:, None] * freq[None, :]
    base = jnp.asarray(np.stack([np.cos(start), np.sin(start)]).astype(np.float32))
    local_cos = jnp.asarray(np.cos(local).astype(np.float32))
    local_sin = jnp.asarray(np.sin(local).astype(np.float32))
    f32, bf16 = jnp.float32, jnp.bfloat16
    V, DMA = pltpu.VMEM, pltpu.SemaphoreType.DMA
    window = ROW_BLOCK + 2 * SIDE_SPAN
    scratch = [
        V((tp_size, shard, depth), bf16),
        V((3, depth, col_count), bf16),
        V((col_count, wide), bf16),
        V((rows, PAIR), f32),
        V((rows, PAIR), f32),
        V((rows, col_count), bf16),
        V((rows + 2 * SIDE_SPAN, 2 * col_count), bf16),
        V((3 * groups, rows, PAIR), f32),
        V((sp_size, cls_rows, 3 * col_count), bf16),
        V((rows, 3 * col_count), bf16),
        V((rows, window), f32),
        V((rows, rows), f32),
        V((groups, rows, PAIR), f32),
        V((rows, PAIR), f32),
        V((rows, col_count), bf16),
        V((rows, PAIR), f32),
        V((rows // PAIR, col_count // HEAD_DIM, PAIR), f32),
        V((rows, col_count), bf16),
        V((sp_size, col_count // HEAD_DIM, PAIR), f32),
        V((groups, rows, PAIR), f32),
        V((rows, PAIR), f32),
        V((rows, col_count), bf16),
        V((chips, OUT_SPLITS, shard, width), bf16),
        V((chips, OUT_SPLITS, shard, width), bf16),
        V((chips, OUT_SPLITS, shard, width), bf16),
        V((chips, OUT_SPLITS, shard, width), bf16),
        V((chips, OUT_SPLITS, shard, width), bf16),
        V((OUT_SPLITS, shard, width), bf16),
        DMA((5,)),
        DMA((1,)), DMA((1,)),
        DMA((chips, SPLITS)), DMA((chips, SPLITS)),
        DMA((chips, SPLITS)), DMA((chips, SPLITS)),
        DMA((chips, sp_size)), DMA((chips, sp_size)),
        DMA((2,)), DMA((2,)),
        DMA((groups, sp_size)), DMA((groups, sp_size)),
        DMA((sp_size,)), DMA((sp_size,)),
        DMA((chips, OUT_SPLITS)), DMA((chips, OUT_SPLITS)),
        DMA((chips, OUT_SPLITS)), DMA((chips, OUT_SPLITS)),
    ]
    any_spec = pl.BlockSpec(memory_space=pl.ANY)
    vmem = pl.BlockSpec(memory_space=pltpu.VMEM)
    return pl.pallas_call(
        functools.partial(class_kernel, sp_size, tp_size, col_count),
        out_shape=(
            jax.ShapeDtypeStruct((shard, wide), bf16),
            jax.ShapeDtypeStruct((col_count // HEAD_DIM, rows), f32),
        ),
        in_specs=[any_spec] * 5 + [vmem] * 3,
        out_specs=(vmem, vmem),
        scratch_shapes=scratch,
        compiler_params=pltpu.CompilerParams(
            collective_id=0, has_side_effects=True, vmem_limit_bytes=66 * 1024 * 1000
        ),
        name="dilated_layer",
    )(tokens_in, w_query, w_key, w_value, w_out, base, local_cos, local_sin)


def solution(mesh):
    in_specs = (P(("sp", "tp"), None), P(None, "tp"), P(None, "tp"), P(None, "tp"), P("tp", None))
    out_specs = (P(("sp", "tp"), None), P("tp", "sp"))
    sp_size, tp_size = mesh.shape["sp"], mesh.shape["tp"]

    def body(*args):
        rows = args[0].shape[0] * tp_size
        whole_class = (
            MIDDLE_DILATION % sp_size == 0
            and rows % (sp_size * ROW_BLOCK // 4) == 0
            and tp_size % 2 == 0
            and tp_size > 2
            and WIDEST_DILATION % sp_size == 0
            and PAIR % (rows // sp_size) == 0
        )
        if whole_class:
            return fused(sp_size, tp_size, *args)
        return per_device(*args)

    return jax.shard_map(body, mesh=mesh, in_specs=in_specs, out_specs=out_specs, check_vma=False)
```

profile of v0, /device:TPU:0, one launch (start us, length us, event | category | flops | bytes accessed | tf_op | source)
XLA Modules:
  0.0 104.8 jit_solution(14083279360519466100)
XLA Ops:
  0.6 100.5 %dilated_layer.1 = (bf16[128,4096]{1,0:T(8,128)(2,1)}, f32[8,512]{1,0:T(8,128)}) custom-call(bf16[128,4096]{1,0:T(8,128)(2,1)} %x_hbm.1, bf16[4096,512]{1,0:T(8,128)(2,1)} %wq_hbm.1, bf16[4096,512]{1,0:T(8,128)(2,1)} %wk_hbm.1, bf16[4096,512]{1,0:T(8,128)(2,1)} %wv_hbm.1, bf16[512,4096]{1,0:T(8,128)(2,1)} %wo_hbm.1, f32[2,8,128]{2,1,0:T(8,128)} %constant.6.clone.base_ref, ...), custom_call_target="tpu_custom_call" | custom-call | tf_op jit(solution)/shard_map/dilated_layer/pallas_call | solution.py:646
  101.1 2.3 %copy.12 = bf16[128,4096]{1,0:T(8,128)(2,1)} copy(bf16[128,4096]{1,0:T(8,128)(2,1)} %get-tuple-element.4) | data formatting | bytes 2097152
  103.4 1.3 %copy.13 = f32[8,512]{1,0:T(8,128)} copy(f32[8,512]{1,0:T(8,128)} %get-tuple-element.5) | data formatting | bytes 32768
where the time goes:
time: 105 us
  Pallas kernels  101 us (96%)
  local copies, waits for them, and re-layouts  3.61 us (3%)
    pallas_call x1, Pallas kernels, fused(): pl.pallas_call(functools.partial(class_kernel, sp_size, tp_size, col_coun...  101 us
    unnamed x2, local copies, waits for them, and re-layouts  3.61 us

commit v1 on v0

v1 whole, which is shorter than its diff:
```python
import functools

import jax
import jax.numpy as jnp
import numpy as np
from jax import lax
from jax.experimental import pallas as pl
from jax.experimental.pallas import tpu as pltpu
from jax.sharding import PartitionSpec as P

HEAD_DIM = 64
SIDE_SPAN = 64
MIDDLE_DILATION = 8
WIDEST_DILATION = 64


ROTARY_BASE = 500000.0
NEGATIVE = -1e30


def shifted(block, axis, distance):
    devices = range(lax.axis_size(axis))
    route = [(i - distance, i) for i in devices if i - distance in devices]
    return lax.ppermute(block, axis, route)


def rotate(block, positions):
    half_size = block.shape[-1] // 2
    freq = 1.0 / ROTARY_BASE ** (jnp.arange(half_size, dtype=jnp.float32) / half_size)
    angle = positions[:, None] * freq[None, :]
    cosine = jnp.cos(angle)[:, None, :]
    sine = jnp.sin(angle)[:, None, :]
    front = block[..., :half_size]
    back = block[..., half_size:]
    return jnp.concatenate([front * cosine - back * sine, back * cosine + front * sine], axis=-1)


def pattern_attend(query, keys, values, lead_rows, dilation_step, low_row, high_row):
    rows_total, head_count, head_size = query.shape
    class_len = rows_total // dilation_step
    first_class = lead_rows // dilation_step - SIDE_SPAN
    class_q = query.reshape(class_len, dilation_step, head_count, head_size)
    class_k = keys.reshape(keys.shape[0] // dilation_step, dilation_step, head_count, head_size)
    class_v = values.reshape(values.shape[0] // dilation_step, dilation_step, head_count, head_size)
    sub_k = class_k[first_class : first_class + class_len + 2 * SIDE_SPAN]
    sub_v = class_v[first_class : first_class + class_len + 2 * SIDE_SPAN]
    if class_len <= SIDE_SPAN:
        block_len = class_len
        block_count = 1
        win_k = sub_k[None]
        win_v = sub_v[None]
        blocks_q = class_q[None]
    else:
        block_len = SIDE_SPAN
        block_count = class_len // SIDE_SPAN
        part_k = sub_k.reshape(block_count + 2, SIDE_SPAN, dilation_step, head_count, head_size)
        part_v = sub_v.reshape(block_count + 2, SIDE_SPAN, dilation_step, head_count, head_size)
        win_k = jnp.concatenate([part_k[:-2], part_k[1:-1], part_k[2:]], axis=1)
        win_v = jnp.concatenate([part_v[:-2], part_v[1:-1], part_v[2:]], axis=1)
        blocks_q = class_q.reshape(block_count, SIDE_SPAN, dilation_step, head_count, head_size)
    width = block_len + 2 * SIDE_SPAN
    scores = jnp.einsum("nasht,nksht->nshak", blocks_q, win_k, preferred_element_type=jnp.float32)
    scores = scores * head_size ** (-0.5)
    q_index = jnp.arange(block_len, dtype=jnp.int32)
    k_index = jnp.arange(width, dtype=jnp.int32)
    b_index = jnp.arange(block_count, dtype=jnp.int32)
    s_index = jnp.arange(dilation_step, dtype=jnp.int32)
    in_band = jnp.abs(k_index[None, :] - SIDE_SPAN - q_index[:, None]) <= SIDE_SPAN
    key_position = (
        (first_class + b_index[:, None] * block_len + k_index[None, :]) * dilation_step
    )[:, None, :] + s_index[None, :, None]
    is_valid = (key_position >= low_row) & (key_position < high_row)
    keep_mask = in_band[None, None, None] & is_valid[:, :, None, None, :]
    scores = jnp.where(keep_mask, scores, NEGATIVE)
    maxima = jnp.max(scores, axis=-1, keepdims=True)
    expo = jnp.exp(scores - maxima)
    totals = jnp.sum(expo, axis=-1)
    numerator = jnp.einsum(
        "nshak,nksht->nasht", expo.astype(jnp.bfloat16), win_v, preferred_element_type=jnp.float32
    )
    totals_t = jnp.transpose(totals, (0, 3, 1, 2))
    result = (
        (numerator / totals_t[..., None])
        .astype(jnp.bfloat16)
        .reshape(rows_total, head_count, head_size)
    )
    log_sum = jnp.transpose(maxima[..., 0] + jnp.log(totals), (0, 3, 1, 2)).reshape(
        rows_total, head_count
    )
    return (result, log_sum)


def combine(results):
    sums = jnp.stack([item[1] for item in results], axis=0)
    peak = jnp.max(sums, axis=0)
    share = jnp.exp(sums - peak[None])
    weight_sum = share[0] + share[1] + share[2]
    accum = share[0][..., None] * results[0][0].astype(jnp.float32)
    accum = accum + share[1][..., None] * results[1][0].astype(jnp.float32)
    accum = accum + share[2][..., None] * results[2][0].astype(jnp.float32)
    attended = (accum / weight_sum[..., None]).astype(jnp.bfloat16)
    return (attended, peak + jnp.log(weight_sum))


def per_device(tokens_in, w_query, w_key, w_value, w_out):
    col_count = w_query.shape[1]
    head_count = col_count // HEAD_DIM
    piece = lax.all_gather(tokens_in, "tp", axis=0, tiled=True)
    projected = jnp.concatenate(
        [
            jnp.dot(piece, w_query, preferred_element_type=jnp.float32),
            jnp.dot(piece, w_key, preferred_element_type=jnp.float32),
            jnp.dot(piece, w_value, preferred_element_type=jnp.float32),
        ],
        axis=1,
    )
    rows_total = projected.shape[0]
    sp_size = lax.axis_size("sp")
    sp_place = lax.axis_index("sp")
    positions = (sp_place * rows_total + jnp.arange(rows_total, dtype=jnp.int32)).astype(
        jnp.float32
    )
    shape3 = (rows_total, head_count, HEAD_DIM)
    query = rotate(projected[:, :col_count].reshape(shape3), positions).astype(jnp.bfloat16)
    keys = rotate(projected[:, col_count : 2 * col_count].reshape(shape3), positions).astype(
        jnp.bfloat16
    )
    values = projected[:, 2 * col_count :].astype(jnp.bfloat16).reshape(shape3)
    per_device_span = -(-(SIDE_SPAN * MIDDLE_DILATION) // rows_total)
    earlier_k = []
    earlier_v = []
    before_k, before_v = shifted((keys, values), "sp", 1)
    after_k, after_v = shifted((keys, values), "sp", -1)
    earlier_k.insert(0, before_k)
    earlier_v.insert(0, before_v)
    later_k = [after_k]
    later_v = [after_v]
    key_buf = jnp.concatenate(earlier_k + [keys] + later_k, axis=0)
    value_buf = jnp.concatenate(earlier_v + [values] + later_v, axis=0)
    lead_rows = per_device_span * rows_total
    low_row = lead_rows - sp_place * rows_total
    key_buf, value_buf, lead_rows, low_row, high_row = (
        key_buf,
        value_buf,
        lead_rows,
        low_row,
        low_row + sp_size * rows_total,
    )
    results = [
        pattern_attend(query, key_buf, value_buf, lead_rows, dilation_step, low_row, high_row)
        for dilation_step in (1, MIDDLE_DILATION)
    ]
    class_stride = WIDEST_DILATION // sp_size
    border_extent = SIDE_SPAN * class_stride
    class_shape = (rows_total // sp_size, sp_size, head_count, HEAD_DIM)
    parts = (
        lax.all_to_all(query.reshape(class_shape), "sp", split_axis=1, concat_axis=0, tiled=True),
        lax.all_to_all(keys.reshape(class_shape), "sp", split_axis=1, concat_axis=0, tiled=True),
        lax.all_to_all(values.reshape(class_shape), "sp", split_axis=1, concat_axis=0, tiled=True),
    )
    item_heads = parts[0].shape[2]
    flat = [item.reshape(rows_total, item_heads, HEAD_DIM) for item in parts]
    pad_k = jnp.pad(flat[1], ((border_extent, border_extent), (0, 0), (0, 0)))
    pad_v = jnp.pad(flat[2], ((border_extent, border_extent), (0, 0), (0, 0)))
    result, log_sum = pattern_attend(
        flat[0],
        pad_k,
        pad_v,
        border_extent,
        class_stride,
        border_extent,
        border_extent + rows_total,
    )
    result_back = lax.all_to_all(
        result.reshape(rows_total, 1, item_heads, HEAD_DIM),
        "sp",
        split_axis=0,
        concat_axis=1,
        tiled=True,
    )
    sum_back = lax.all_to_all(
        log_sum.reshape(rows_total, 1, item_heads), "sp", split_axis=0, concat_axis=1, tiled=True
    )
    results.append((result_back.reshape(shape3), sum_back.reshape(rows_total, head_count)))
    attended, log_weight = combine(results)
    flat_out = attended.reshape(rows_total, col_count)
    mixed = lax.psum_scatter(
        jnp.dot(flat_out, w_out, preferred_element_type=jnp.float32).astype(jnp.bfloat16),
        "tp",
        scatter_dimension=0,
        tiled=True,
    )
    return (mixed, jnp.transpose(log_weight, (1, 0)))


MESH_ID = pl.DeviceIdType.MESH
PAIR = 2 * HEAD_DIM
ROW_BLOCK = 128
SPLITS = 2
OUT_SPLITS = 4
SEGMENTS = 4
K, V, Q = 0, 1, 2
UNITS = ((0, (K, V)), (1, (K, V)), (2, (K, V, Q)), (0, (Q,)), (3, (K, V)), (3, (Q,)), (1, (Q,)))


def class_kernel(
    sp_size, tp_size, col_count,
    x_hbm, wq_hbm, wk_hbm, wv_hbm, wo_hbm, table_hbm,
    out_ref, logw_ref,
    x_all, w_all, wo, table, cos_t, sin_t, q_c, kv_ext, pf, cls_send, cls_recv,
    bias_near, bias_class, o_near, lse_near, cls_o, cls_lse, lse_out, ret, ret_lse, ret_f, lse_f, logw_far,
    att, part_out, part_in, cross_out, cross_in, keep_b, keep_d, own_out, own_in,
    load_sem, own_send, own_recv, far_send, far_recv, fwd_send, fwd_recv,
    a2a_send, a2a_recv, halo_send, halo_recv, back_send, back_recv, lback_send, lback_recv,
    ex_send, ex_recv, cr_send, cr_recv, ox_send, ox_recv,
):
    sp = lax.axis_index("sp")
    tp = lax.axis_index("tp")
    chip = tp // 2
    core = tp % 2
    partner = chip * 2 + (1 - core)
    far_same = (1 - chip) * 2 + core
    far_other = (1 - chip) * 2 + (1 - core)
    shard = x_hbm.shape[0]
    rows = shard * tp_size
    piece = shard // SPLITS
    group_count = col_count // PAIR
    head_count = col_count // HEAD_DIM
    share = shard // sp_size
    f32, bf16 = jnp.float32, jnp.bfloat16

    offsets = sorted(range(1, sp_size), key=lambda off: (abs(off - sp_size // 2), off))

    spans = (
        ((tp, 0, shard),),
        ((partner, 0, shard),),
        ((far_same, 0, piece), (far_other, 0, piece)),
        ((far_same, piece, piece), (far_other, piece, piece)),
    )

    def row_of(s, a, c):
        return pl.multiple_of(s * shard + a, c)

    load_table = pltpu.make_async_copy(table_hbm, table, load_sem.at[0])
    load_x = pltpu.make_async_copy(x_hbm, x_all.at[tp], load_sem.at[1])
    load_w = [
        pltpu.make_async_copy(w, w_all.at[n], load_sem.at[2 + n])
        for n, w in enumerate((wk_hbm, wv_hbm, wq_hbm))
    ]
    load_out = pltpu.make_async_copy(wo_hbm, wo, load_sem.at[5])
    load_x.start()
    load_table.start()
    for item in load_w:
        item.start()

    barrier = pltpu.get_barrier_semaphore()
    pl.semaphore_signal(barrier, inc=1, device_id={"tp": partner}, device_id_type=MESH_ID)
    pl.semaphore_signal(barrier, inc=1, device_id={"tp": far_same}, device_id_type=MESH_ID)
    for off in offsets:
        pl.semaphore_signal(
            barrier, inc=1, device_id={"sp": (sp + off) % sp_size}, device_id_type=MESH_ID
        )
    pl.semaphore_wait(barrier, 2 + (sp_size - 1))

    def remote(src, dst, send, recv, **where):
        return pltpu.make_async_remote_copy(
            src_ref=src, dst_ref=dst, send_sem=send, recv_sem=recv,
            device_id=where, device_id_type=MESH_ID,
        )

    waits = []

    def launch(item):
        item.start()
        waits.append(item)
        return item

    far = []
    for k in range(SPLITS):
        span = pl.ds(k * piece, piece)
        far.append(
            launch(
                remote(
                    x_hbm.at[span], x_all.at[tp, span], far_send.at[k], far_recv.at[k], tp=far_same
                )
            )
        )
    own = launch(remote(x_hbm, x_all.at[tp], own_send.at[0], own_recv.at[0], tp=partner))
    load_out.start()

    lane = lax.broadcasted_iota(jnp.int32, (1, PAIR), 1)
    front = lane % HEAD_DIM < HEAD_DIM // 2
    first_head = lane < HEAD_DIM
    sign = jnp.where(front, -1.0, 1.0).astype(f32)
    load_table.wait()
    base_cos = table[0, pl.ds(rows + sp, 1), :]
    base_sin = table[1, pl.ds(rows + sp, 1), :]
    for r0 in range(0, rows, ROW_BLOCK):
        lc = table[0, r0 : r0 + ROW_BLOCK]
        ls = table[1, r0 : r0 + ROW_BLOCK]
        cos_t[r0 : r0 + ROW_BLOCK] = lc * base_cos - ls * base_sin
        sin_t[r0 : r0 + ROW_BLOCK] = (ls * base_cos + lc * base_sin) * sign

    window = ROW_BLOCK + 2 * SIDE_SPAN
    mid_step = MIDDLE_DILATION // sp_size
    wide_step = WIDEST_DILATION // sp_size
    per_source = rows // sp_size
    half_share = share // 2

    def place_of(seg, index):
        source = index // share
        j = index % share
        if seg < 2:
            inner = spans[seg][0][0] * share + j
        else:
            inner = jnp.where(
                j < half_share,
                far_same * share + (seg - 2) * half_share + j,
                far_other * share + (seg - 3) * half_share + j,
            )
        return source * per_source + inner

    def build_bias():
        near_i = lax.broadcasted_iota(jnp.int32, (ROW_BLOCK, window), 0)
        near_j = lax.broadcasted_iota(jnp.int32, (ROW_BLOCK, window), 1)
        near_band = jnp.abs(near_j - SIDE_SPAN - near_i) <= SIDE_SPAN
        for r0 in range(0, rows, ROW_BLOCK):
            key_pos = sp * rows + r0 + near_j - SIDE_SPAN
            good = near_band & (key_pos >= 0) & (key_pos < sp_size * rows)
            bias_near[r0 : r0 + ROW_BLOCK] = jnp.where(good, 0.0, NEGATIVE)
        for a in range(SEGMENTS):
            q_place = place_of(a, lax.broadcasted_iota(jnp.int32, (ROW_BLOCK, 1), 0))
            for b in range(SEGMENTS):
                k_place = place_of(b, lax.broadcasted_iota(jnp.int32, (1, ROW_BLOCK), 1))
                gap = jnp.abs(q_place - k_place)
                mid = (gap % mid_step == 0) & (gap <= SIDE_SPAN * mid_step)
                wide = (gap % wide_step == 0) & (gap <= SIDE_SPAN * wide_step)
                bias_class[
                    a * ROW_BLOCK : (a + 1) * ROW_BLOCK, b * ROW_BLOCK : (b + 1) * ROW_BLOCK
                ] = jnp.where(
                    mid & wide, float(np.log(2.0)), jnp.where(mid | wide, 0.0, NEGATIVE)
                )

    def turn(x, cos, sin):
        swapped = jnp.where(
            front, pltpu.roll(x, PAIR - HEAD_DIM // 2, 1), pltpu.roll(x, HEAD_DIM // 2, 1)
        )
        return x * cos + swapped * sin

    def project(seg, n):
        if len(spans[seg]) == 1:
            left = x_all[spans[seg][0][0]]
        else:
            left = jnp.concatenate([x_all[s, pl.ds(a, c)] for s, a, c in spans[seg]], axis=0)
        full = jnp.dot(left, w_all[n], preferred_element_type=f32)
        at = 0
        for s, a, c in spans[seg]:
            r0 = row_of(s, a, c)
            if n != V:
                cos = cos_t[pl.ds(r0, c)]
                sin = sin_t[pl.ds(r0, c)]
            for g in range(group_count):
                part = full[at : at + c, g * PAIR : (g + 1) * PAIR]
                if n != V:
                    part = turn(part, cos, sin)
                pf[n * group_count + g, seg * shard + at : seg * shard + at + c, :] = part
                low = part.astype(bf16)
                if n == Q:
                    q_c[pl.ds(r0, c), g * PAIR : (g + 1) * PAIR] = low
                else:
                    kv_ext[
                        pl.ds(r0 + SIDE_SPAN, c),
                        n * col_count + g * PAIR : n * col_count + (g + 1) * PAIR,
                    ] = low
            at += c

    a2a = {}

    def scatter(unit):
        seg, names = UNITS[unit]
        span = slice(seg * share, (seg + 1) * share)
        cols = slice(names[0] * col_count, (names[-1] + 1) * col_count)

        def one(r, carry):
            for g in range(names[0] * group_count, (names[-1] + 1) * group_count):
                cls_send[r, span, g * PAIR : (g + 1) * PAIR] = pf[
                    g, pl.ds(seg * shard + r, share, stride=sp_size), :
                ].astype(bf16)
            return carry

        lax.fori_loop(0, sp_size, one, 0)
        mine = pl.ds(pl.multiple_of(seg * shard + sp * share, share), share)
        for off in offsets:
            dest = (sp + off) % sp_size
            a2a[unit, off] = launch(
                remote(
                    cls_send.at[dest, span, cols], cls_recv.at[mine, cols],
                    a2a_send.at[unit, off], a2a_recv.at[unit, off], sp=dest,
                )
            )
        cls_recv[mine, cols] = cls_send[sp, span, cols]

    def gathered(*units):
        for unit in units:
            for off in offsets:
                a2a[unit, off].wait_recv()

    def edge(which, n):
        src = pl.multiple_of(SIDE_SPAN + which * (rows - SIDE_SPAN), SIDE_SPAN)
        dst = pl.multiple_of((1 - which) * (rows + SIDE_SPAN), SIDE_SPAN)
        return launch(
            remote(
                kv_ext.at[pl.ds(src, SIDE_SPAN)], kv_ext.at[pl.ds(dst, SIDE_SPAN)],
                halo_send.at[n], halo_recv.at[n], sp=(sp + sp_size - 1 + 2 * which) % sp_size,
            )
        )

    load_x.wait()
    load_w[K].wait()
    project(0, K)
    load_w[V].wait()
    project(0, V)
    scatter(0)
    own.wait_recv()
    project(1, K)
    project(1, V)
    scatter(1)
    halo_early = edge(chip, 0)
    load_w[Q].wait()
    project(0, Q)
    project(1, Q)

    fwd = []
    for k in range(SPLITS):
        span = pl.ds(k * piece, piece)
        far[k].wait_recv()
        fwd.append(
            launch(
                remote(
                    x_all.at[far_same, span], x_all.at[far_same, span],
                    fwd_send.at[k], fwd_recv.at[k], tp=partner,
                )
            )
        )
        if k == 0:
            build_bias()
        fwd[k].wait_recv()
        project(2 + k, K)
        project(2 + k, V)
        if k == 0:
            project(2, Q)
            scatter(2)
            scatter(3)
        else:
            scatter(4)
            project(3, Q)
            scatter(5)
    halo_late = edge(1 - chip, 1)

    lane_wide = lax.broadcasted_iota(jnp.int32, (ROW_BLOCK, PAIR), 1)
    scale = HEAD_DIM ** (-0.5)

    def attend(query, keys, values, bias):
        outs, sums = [], []
        for half in range(2):
            pick = first_head if half == 0 else jnp.logical_not(first_head)
            q = jnp.where(pick, query.astype(f32) * scale, 0.0).astype(bf16)
            s = lax.dot_general(q, keys, (((1,), (1,)), ((), ())), preferred_element_type=f32)
            s = s + bias
            top = jnp.max(s, axis=1, keepdims=True)
            e = jnp.exp(s - top)
            total = jnp.sum(e, axis=1, keepdims=True)
            o = jnp.dot(e.astype(bf16), values, preferred_element_type=f32)
            outs.append(o / total)
            sums.append(top + jnp.log(total))
        return jnp.where(first_head, outs[0], outs[1]), sums

    def keep_sums(ref, span, g, sums):
        kept = ref[span]
        kept = jnp.where(lane_wide == 2 * g, sums[0], kept)
        ref[span] = jnp.where(lane_wide == 2 * g + 1, sums[1], kept)

    def near(shards):
        def pair(g, carry):
            c0 = pl.multiple_of(g * PAIR, PAIR)
            for s in shards:
                r0 = row_of(s, 0, shard)
                span = pl.ds(r0, ROW_BLOCK)
                o, sums = attend(
                    q_c[span, pl.ds(c0, PAIR)],
                    kv_ext[pl.ds(r0, window), pl.ds(c0, PAIR)],
                    kv_ext[pl.ds(r0, window), pl.ds(c0 + col_count, PAIR)],
                    bias_near[span],
                )
                o_near[g, span, :] = o
                keep_sums(lse_near, span, g, sums)
            return carry

        lax.fori_loop(0, group_count, pair, 0)

    my_share = pl.ds(pl.multiple_of(sp * share, share), share)
    back, lback = {}, {}

    def class_attend(seg):
        span = slice(seg * shard, (seg + 1) * shard)

        def block(g):
            c0 = pl.multiple_of(g * PAIR, PAIR)
            o, sums = attend(
                cls_recv[span, pl.ds(c0 + Q * col_count, PAIR)],
                cls_recv[:, pl.ds(c0 + K * col_count, PAIR)],
                cls_recv[:, pl.ds(c0 + V * col_count, PAIR)],
                bias_class[span],
            )
            cls_o[span, pl.ds(c0, PAIR)] = o.astype(bf16)
            keep_sums(cls_lse, span, g, sums)

        def two(i, carry):
            block(2 * i)
            block(2 * i + 1)
            return carry

        lax.fori_loop(0, group_count // 2, two, 0)
        lse_out[seg] = jnp.transpose(cls_lse[span])[:head_count]
        for off in offsets:
            dest = (sp + off) % sp_size
            part = pl.ds(pl.multiple_of(seg * shard + dest * share, share), share)
            back[seg, off] = launch(
                remote(
                    cls_o.at[part], ret.at[seg, my_share],
                    back_send.at[seg, off], back_recv.at[seg, off], sp=dest,
                )
            )
            lback[seg, off] = launch(
                remote(
                    lse_out.at[seg], ret_lse.at[seg, sp],
                    lback_send.at[seg, off], lback_recv.at[seg, off], sp=dest,
                )
            )
        mine = pl.ds(pl.multiple_of(seg * shard + sp * share, share), share)
        ret[seg, my_share] = cls_o[mine]
        ret_lse[seg, sp] = lse_out[seg]

    head_lane = lax.broadcasted_iota(jnp.int32, (head_count, PAIR), 1)

    def gather_rows(ref, seg):
        return jnp.concatenate([ref[pl.ds(row_of(s, a, c), c)] for s, a, c in spans[seg]], axis=0)

    def combine(seg):
        for off in offsets:
            lback[seg, off].wait_recv()
        flat = jnp.zeros((head_count, PAIR), f32)
        for r in range(sp_size):
            moved = pltpu.roll(ret_lse[seg, r], (r - sp + sp_size) % sp_size * share, 1)
            flat = jnp.where(head_lane // share == r, moved, flat)
        tall = jnp.transpose(
            jnp.concatenate([flat, jnp.zeros((PAIR - head_count, PAIR), f32)], axis=0)
        )
        for r in range(sp_size):
            lse_f[pl.ds(r, share, stride=sp_size), :] = tall[r * share : (r + 1) * share]
        for off in offsets:
            back[seg, off].wait_recv()
        for g in range(group_count):
            for r in range(sp_size):
                ret_f[g, pl.ds(r, share, stride=sp_size), :] = ret[
                    seg, r * share : (r + 1) * share, g * PAIR : (g + 1) * PAIR
                ].astype(f32)
        la = gather_rows(lse_near, seg)
        lb = lse_f[...]
        peak = jnp.maximum(la, lb)
        ea = jnp.exp(la - peak)
        eb = jnp.exp(lb - peak)
        total = ea + eb
        logw = jnp.transpose(peak + jnp.log(total))[:head_count]
        if seg < 2:
            logw_ref[:, pl.ds(row_of(*spans[seg][0]), shard)] = logw
        else:
            logw_far[seg - 2] = logw
        ea = ea / total
        eb = eb / total
        for g in range(group_count):
            wa = jnp.where(first_head, ea[:, 2 * g : 2 * g + 1], ea[:, 2 * g + 1 : 2 * g + 2])
            wb = jnp.where(first_head, eb[:, 2 * g : 2 * g + 1], eb[:, 2 * g + 1 : 2 * g + 2])
            mixed = wa * gather_rows(o_near.at[g], seg) + wb * ret_f[g]
            att[seg, :, g * PAIR : (g + 1) * PAIR] = mixed.astype(bf16)

    width = wo.shape[1] // OUT_SPLITS

    def product(seg, n):
        return jnp.dot(
            att[seg], wo[:, n * width : (n + 1) * width], preferred_element_type=f32
        ).astype(bf16)

    exch, cross, own_exch = {}, {}, {}

    def relay(k, n):
        exch[k, n].wait_recv()
        cross_out[k, n] = (keep_b[k, n].astype(f32) + part_in[k, n].astype(f32)).astype(bf16)
        cross[k, n] = launch(
            remote(
                cross_out.at[k, n], cross_in.at[k, n], cr_send.at[k, n], cr_recv.at[k, n],
                tp=far_same,
            )
        )

    def out_far(k):
        for n in range(OUT_SPLITS):
            both = product(2 + k, n)
            part_out[k, n] = both[piece:]
            exch[k, n] = launch(
                remote(
                    part_out.at[k, n], part_in.at[k, n], ex_send.at[k, n], ex_recv.at[k, n],
                    tp=partner,
                )
            )
            keep_b[k, n] = both[:piece]
            if n:
                relay(k, n - 1)
        relay(k, OUT_SPLITS - 1)

    lse_near[...] = jnp.zeros_like(lse_near)
    cls_lse[...] = jnp.zeros_like(cls_lse)
    halo_early.wait_recv()
    near((far_same, far_other))
    gathered(0, 1, 2, 4)
    class_attend(2)
    scatter(6)
    gathered(5)
    class_attend(3)
    load_out.wait()
    combine(2)
    out_far(0)
    combine(3)
    out_far(1)
    first_half = head_lane < piece
    swap = [pltpu.roll(logw_far[k], piece, 1) for k in range(SPLITS)]
    logw_ref[:, pl.ds(row_of(far_same, 0, shard), shard)] = jnp.where(
        first_half, logw_far[0], swap[1]
    )
    logw_ref[:, pl.ds(row_of(far_other, 0, shard), shard)] = jnp.where(
        first_half, swap[0], logw_far[1]
    )
    gathered(3)
    class_attend(0)
    gathered(6)
    class_attend(1)
    halo_late.wait_recv()
    near((tp, partner))
    combine(1)
    for n in range(OUT_SPLITS):
        own_out[n] = product(1, n)
        own_exch[n] = launch(
            remote(own_out.at[n], own_in.at[n], ox_send.at[n], ox_recv.at[n], tp=partner)
        )
    combine(0)
    for n in range(OUT_SPLITS):
        keep_d[n] = product(0, n).astype(f32)
    for n in range(OUT_SPLITS):
        own_exch[n].wait_recv()
        keep_d[n] = keep_d[n] + own_in[n].astype(f32)
    for k in range(SPLITS):
        for n in range(OUT_SPLITS):
            cross[k, n].wait_recv()
            out_ref[k * piece : (k + 1) * piece, n * width : (n + 1) * width] = (
                keep_d[n, k * piece : (k + 1) * piece] + cross_in[k, n].astype(f32)
            ).astype(bf16)

    for item in waits:
        item.wait_send()


def fused(sp_size, tp_size, tokens_in, w_query, w_key, w_value, w_out):
    shard, depth = tokens_in.shape
    col_count = w_query.shape[1]
    rows = shard * tp_size
    groups = col_count // PAIR
    heads = col_count // HEAD_DIM
    share = shard // sp_size
    piece = shard // SPLITS
    wide = w_out.shape[1]
    width = wide // OUT_SPLITS
    half = HEAD_DIM // 2
    freq = 1.0 / ROTARY_BASE ** (np.arange(half) / half)
    freq = np.tile(freq, PAIR // half)
    start = np.concatenate([np.arange(rows), np.arange(sp_size) * rows])
    angle = start[:, None] * freq[None, :]
    table = jnp.asarray(np.stack([np.cos(angle), np.sin(angle)]).astype(np.float32))
    f32, bf16 = jnp.float32, jnp.bfloat16
    V_, DMA = pltpu.VMEM, pltpu.SemaphoreType.DMA
    window = ROW_BLOCK + 2 * SIDE_SPAN
    scratch = [
        V_((tp_size, shard, depth), bf16),
        V_((3, depth, col_count), bf16),
        V_((col_count, wide), bf16),
        V_(table.shape, f32),
        V_((rows, PAIR), f32),
        V_((rows, PAIR), f32),
        V_((rows, col_count), bf16),
        V_((rows + 2 * SIDE_SPAN, 2 * col_count), bf16),
        V_((3 * groups, rows, PAIR), f32),
        V_((sp_size, SEGMENTS * share, 3 * col_count), bf16),
        V_((rows, 3 * col_count), bf16),
        V_((rows, window), f32),
        V_((rows, rows), f32),
        V_((groups, rows, PAIR), f32),
        V_((rows, PAIR), f32),
        V_((rows, col_count), bf16),
        V_((rows, PAIR), f32),
        V_((SEGMENTS, heads, PAIR), f32),
        V_((SEGMENTS, shard, col_count), bf16),
        V_((SEGMENTS, sp_size, heads, PAIR), f32),
        V_((groups, shard, PAIR), f32),
        V_((shard, PAIR), f32),
        V_((SPLITS, heads, PAIR), f32),
        V_((SEGMENTS, shard, col_count), bf16),
        V_((SPLITS, OUT_SPLITS, piece, width), bf16),
        V_((SPLITS, OUT_SPLITS, piece, width), bf16),
        V_((SPLITS, OUT_SPLITS, piece, width), bf16),
        V_((SPLITS, OUT_SPLITS, piece, width), bf16),
        V_((SPLITS, OUT_SPLITS, piece, width), bf16),
        V_((OUT_SPLITS, shard, width), f32),
        V_((OUT_SPLITS, shard, width), bf16),
        V_((OUT_SPLITS, shard, width), bf16),
        DMA((6,)),
        DMA((1,)), DMA((1,)),
        DMA((SPLITS,)), DMA((SPLITS,)),
        DMA((SPLITS,)), DMA((SPLITS,)),
        DMA((len(UNITS), sp_size)), DMA((len(UNITS), sp_size)),
        DMA((2,)), DMA((2,)),
        DMA((SEGMENTS, sp_size)), DMA((SEGMENTS, sp_size)),
        DMA((SEGMENTS, sp_size)), DMA((SEGMENTS, sp_size)),
        DMA((SPLITS, OUT_SPLITS)), DMA((SPLITS, OUT_SPLITS)),
        DMA((SPLITS, OUT_SPLITS)), DMA((SPLITS, OUT_SPLITS)),
        DMA((OUT_SPLITS,)), DMA((OUT_SPLITS,)),
    ]
    hbm = pl.BlockSpec(memory_space=pltpu.HBM)
    vmem = pl.BlockSpec(memory_space=pltpu.VMEM)
    return pl.pallas_call(
        functools.partial(class_kernel, sp_size, tp_size, col_count),
        out_shape=(
            jax.ShapeDtypeStruct((shard, wide), bf16),
            jax.ShapeDtypeStruct((heads, rows), f32),
        ),
        in_specs=[hbm] * 6,
        out_specs=(vmem, vmem),
        scratch_shapes=scratch,
        compiler_params=pltpu.CompilerParams(
            collective_id=0, has_side_effects=True, vmem_limit_bytes=VMEM_GRANT
        ),
        name="dilated_layer",
    )(tokens_in, w_query, w_key, w_value, w_out, table)


VMEM_GRANT = 52 * 1024 * 1024


def solution(mesh):
    in_specs = (P(("sp", "tp"), None), P(None, "tp"), P(None, "tp"), P(None, "tp"), P("tp", None))
    out_specs = (P(("sp", "tp"), None), P("tp", "sp"))
    sp_size, tp_size = mesh.shape["sp"], mesh.shape["tp"]

    def body(*args):
        shard = args[0].shape[0]
        whole_class = (
            MIDDLE_DILATION % sp_size == 0
            and WIDEST_DILATION % sp_size == 0
            and tp_size == 2 * SPLITS
            and shard == ROW_BLOCK
            and shard % (16 * sp_size) == 0
            and args[1].shape[1] % (2 * PAIR) == 0
        )
        if whole_class:
            return fused(sp_size, tp_size, *args)
        return per_device(*args)

    return jax.shard_map(body, mesh=mesh, in_specs=in_specs, out_specs=out_specs, check_vma=False)
```

time: 105 us -> 88 us (0.84)
  Pallas kernels: 101 us -> 84.6 us
    pallas_call x1, Pallas kernels: 101 us -> 84.6 us  [fused(): pl.pallas_call(functools.partial(class_kernel, sp_size, tp_size, col_coun...]
    unnamed x2 -> x4, local copies, waits for them, and re-layouts: 3.61 us -> 2.62 us
where the time goes in v1:
time: 88 us; the launch traced here: 87.8 us
  Pallas kernels  84.6 us (96%)
  local copies, waits for them, and re-layouts  2.62 us (3%)
    pallas_call x1, Pallas kernels, fused(): pl.pallas_call(functools.partial(class_kernel, sp_size, tp_size, col_coun...  84.6 us
    unnamed x4, local copies, waits for them, and re-layouts  2.62 us

profile of v1, /device:TPU:0, one launch (start us, length us, event | category | flops | bytes accessed | tf_op | source)
XLA Modules:
  0.0 87.8 jit_solution(3087187326408461129)
XLA Ops:
  0.6 0.0 copy-start
  0.6 1.0 %copy-done = f32[2,520,128]{2,1,0:T(8,128)S(1)} copy-done((f32[2,520,128]{2,1,0:T(8,128)S(1)}, f32[2,520,128]{2,1,0:T(8,128)}, u32[]{:S(2)}) %copy-start) | copy-done | bytes 532504
  1.7 84.6 %dilated_layer.1 = (bf16[128,4096]{1,0:T(8,128)(2,1)S(1)}, f32[8,512]{1,0:T(8,128)S(1)}) custom-call(bf16[128,4096]{1,0:T(8,128)(2,1)} %x_hbm.1, bf16[4096,512]{1,0:T(8,128)(2,1)} %wq_hbm.1, bf16[4096,512]{1,0:T(8,128)(2,1)} %wk_hbm.1, bf16[4096,512]{1,0:T(8,128)(2,1)} %wv_hbm.1, bf16[512,4096]{1,0:T(8,128)(2,1)} %wo_hbm.1, f32[2,520,128]{2,1,0:T(8,128)S(1)} %copy-done), custom_call_target="tpu_custom_call" | custom-call | tf_op jit(solution)/shard_map/dilated_layer/pallas_call | solution.py:738
  86.3 1.0 %copy.10 = bf16[128,4096]{1,0:T(8,128)(2,1)} copy(bf16[128,4096]{1,0:T(8,128)(2,1)S(1)} %get-tuple-element.4) | data formatting | bytes 2097152
  87.2 0.6 copy.11
Async XLA Ops:
  0.6 1.0 %copy-start = (f32[2,520,128]{2,1,0:T(8,128)S(1)}, f32[2,520,128]{2,1,0:T(8,128)}, u32[]{:S(2)}) copy-start(f32[2,520,128]{2,1,0:T(8,128)} %constant.2.clone.table_hbm) | copy-start | bytes 1597444

commit v2 on v1

--- a/solution.py
+++ b/solution.py
@@ -200,7 +200,7 @@
 OUT_SPLITS = 4
 SEGMENTS = 4
 K, V, Q = 0, 1, 2
-UNITS = ((0, (K, V)), (1, (K, V)), (2, (K, V, Q)), (0, (Q,)), (3, (K, V)), (3, (Q,)), (1, (Q,)))
+UNITS = ((0, (K, V)), (1, (K, V)), (0, (Q,)), (1, (Q,)), (2, (K, V, Q)), (3, (K, V)), (3, (Q,)))
 
 
 def class_kernel(
@@ -241,7 +241,7 @@
     def row_of(s, a, c):
         return pl.multiple_of(s * shard + a, c)
 
-    load_table = pltpu.make_async_copy(table_hbm, table, load_sem.at[0])
+    load_table = pltpu.make_async_copy(table_hbm.at[0:2], table, load_sem.at[0])
     load_x = pltpu.make_async_copy(x_hbm, x_all.at[tp], load_sem.at[1])
     load_w = [
         pltpu.make_async_copy(w, w_all.at[n], load_sem.at[2 + n])
@@ -374,7 +374,17 @@
                     ] = low
             at += c
 
-    a2a = {}
+    def bulk(ref, send, recv):
+        return remote(ref, ref, send, recv, tp=partner)
+
+    others = (sp_size - 1) * share
+
+    def a2a_total(unit):
+        seg, names = UNITS[unit]
+        cols = slice(names[0] * col_count, (names[-1] + 1) * col_count)
+        return bulk(
+            cls_recv.at[pl.ds(seg * shard, others), cols], a2a_send.at[unit], a2a_recv.at[unit]
+        )
 
     def scatter(unit):
         seg, names = UNITS[unit]
@@ -392,18 +402,16 @@
         mine = pl.ds(pl.multiple_of(seg * shard + sp * share, share), share)
         for off in offsets:
             dest = (sp + off) % sp_size
-            a2a[unit, off] = launch(
-                remote(
-                    cls_send.at[dest, span, cols], cls_recv.at[mine, cols],
-                    a2a_send.at[unit, off], a2a_recv.at[unit, off], sp=dest,
-                )
-            )
+            remote(
+                cls_send.at[dest, span, cols], cls_recv.at[mine, cols],
+                a2a_send.at[unit], a2a_recv.at[unit], sp=dest,
+            ).start()
+        waits.append(a2a_total(unit))
         cls_recv[mine, cols] = cls_send[sp, span, cols]
 
     def gathered(*units):
         for unit in units:
-            for off in offsets:
-                a2a[unit, off].wait_recv()
+            a2a_total(unit).wait_recv()
 
     def edge(which, n):
         src = pl.multiple_of(SIDE_SPAN + which * (rows - SIDE_SPAN), SIDE_SPAN)
@@ -428,7 +436,9 @@
     halo_early = edge(chip, 0)
     load_w[Q].wait()
     project(0, Q)
+    scatter(2)
     project(1, Q)
+    scatter(3)
 
     fwd = []
     for k in range(SPLITS):
@@ -449,13 +459,10 @@
         project(2 + k, V)
         if k == 0:
             project(2, Q)
-            scatter(2)
-            scatter(3)
+            scatter(4)
         else:
-            scatter(4)
+            scatter(5)
             project(3, Q)
-            scatter(5)
-    halo_late = edge(1 - chip, 1)
 
     lane_wide = lax.broadcasted_iota(jnp.int32, (ROW_BLOCK, PAIR), 1)
     scale = HEAD_DIM ** (-0.5)
@@ -499,9 +506,14 @@
         lax.fori_loop(0, group_count, pair, 0)
 
     my_share = pl.ds(pl.multiple_of(sp * share, share), share)
-    back, lback = {}, {}
-
-    def class_attend(seg):
+
+    def back_total(seg):
+        return bulk(ret.at[seg, pl.ds(0, others)], back_send.at[seg], back_recv.at[seg])
+
+    def lback_total(seg):
+        return bulk(ret_lse.at[seg, pl.ds(0, sp_size - 1)], lback_send.at[seg], lback_recv.at[seg])
+
+    def class_attend(seg, groups=None):
         span = slice(seg * shard, (seg + 1) * shard)
 
         def block(g):
@@ -520,46 +532,60 @@
             block(2 * i + 1)
             return carry
 
-        lax.fori_loop(0, group_count // 2, two, 0)
-        lse_out[seg] = jnp.transpose(cls_lse[span])[:head_count]
+        if groups is None:
+            lax.fori_loop(0, group_count // 2, two, 0)
+        else:
+            for g in groups:
+                block(g)
+
+    def send_back(seg, groups):
+        cols = slice(groups[0] * PAIR, (groups[-1] + 1) * PAIR)
         for off in offsets:
             dest = (sp + off) % sp_size
             part = pl.ds(pl.multiple_of(seg * shard + dest * share, share), share)
-            back[seg, off] = launch(
-                remote(
-                    cls_o.at[part], ret.at[seg, my_share],
-                    back_send.at[seg, off], back_recv.at[seg, off], sp=dest,
-                )
-            )
-            lback[seg, off] = launch(
-                remote(
-                    lse_out.at[seg], ret_lse.at[seg, sp],
-                    lback_send.at[seg, off], lback_recv.at[seg, off], sp=dest,
-                )
-            )
+            remote(
+                cls_o.at[part, cols], ret.at[seg, my_share, cols],
+                back_send.at[seg], back_recv.at[seg], sp=dest,
+            ).start()
         mine = pl.ds(pl.multiple_of(seg * shard + sp * share, share), share)
-        ret[seg, my_share] = cls_o[mine]
-        ret_lse[seg, sp] = lse_out[seg]
+        ret[seg, my_share, cols] = cls_o[mine, cols]
+
+    def send_sums(seg):
+        span = slice(seg * shard, (seg + 1) * shard)
+        lse_out[seg] = exchange_blocks(jnp.transpose(cls_lse[span])[:head_count])[:, None, :]
+        for off in offsets:
+            dest = (sp + off) % sp_size
+            remote(
+                lse_out.at[seg, dest], ret_lse.at[seg, sp], lback_send.at[seg], lback_recv.at[seg],
+                sp=dest,
+            ).start()
+        ret_lse[seg, sp] = lse_out[seg, sp]
+        waits.append(back_total(seg))
+        waits.append(lback_total(seg))
 
     head_lane = lax.broadcasted_iota(jnp.int32, (head_count, PAIR), 1)
+
+    head_row = lax.broadcasted_iota(jnp.int32, (head_count, PAIR), 0)
+
+    def exchange_blocks(x):
+        out = x
+        for k in range(1, head_count):
+            moved = pltpu.roll(pltpu.roll(x, k * share, 1), head_count - k, 0)
+            out = jnp.where(head_lane // share == (head_row + k) % head_count, moved, out)
+        return out
 
     def gather_rows(ref, seg):
         return jnp.concatenate([ref[pl.ds(row_of(s, a, c), c)] for s, a, c in spans[seg]], axis=0)
 
     def combine(seg):
-        for off in offsets:
-            lback[seg, off].wait_recv()
-        flat = jnp.zeros((head_count, PAIR), f32)
-        for r in range(sp_size):
-            moved = pltpu.roll(ret_lse[seg, r], (r - sp + sp_size) % sp_size * share, 1)
-            flat = jnp.where(head_lane // share == r, moved, flat)
+        lback_total(seg).wait_recv()
+        flat = exchange_blocks(ret_lse[seg][:, 0, :])
         tall = jnp.transpose(
             jnp.concatenate([flat, jnp.zeros((PAIR - head_count, PAIR), f32)], axis=0)
         )
         for r in range(sp_size):
             lse_f[pl.ds(r, share, stride=sp_size), :] = tall[r * share : (r + 1) * share]
-        for off in offsets:
-            back[seg, off].wait_recv()
+        back_total(seg).wait_recv()
         for g in range(group_count):
             for r in range(sp_size):
                 ret_f[g, pl.ds(r, share, stride=sp_size), :] = ret[
@@ -591,47 +617,62 @@
             att[seg], wo[:, n * width : (n + 1) * width], preferred_element_type=f32
         ).astype(bf16)
 
-    exch, cross, own_exch = {}, {}, {}
+    exch, cross = {}, {}
 
     def relay(k, n):
         exch[k, n].wait_recv()
         cross_out[k, n] = (keep_b[k, n].astype(f32) + part_in[k, n].astype(f32)).astype(bf16)
-        cross[k, n] = launch(
-            remote(
-                cross_out.at[k, n], cross_in.at[k, n], cr_send.at[k, n], cr_recv.at[k, n],
-                tp=far_same,
-            )
-        )
+        cross[k, n] = remote(
+            cross_out.at[k, n], cross_in.at[k, n], cr_send.at[k], cr_recv.at[k, n], tp=far_same
+        )
+        cross[k, n].start()
 
     def out_far(k):
         for n in range(OUT_SPLITS):
             both = product(2 + k, n)
             part_out[k, n] = both[piece:]
-            exch[k, n] = launch(
-                remote(
-                    part_out.at[k, n], part_in.at[k, n], ex_send.at[k, n], ex_recv.at[k, n],
-                    tp=partner,
-                )
+            exch[k, n] = remote(
+                part_out.at[k, n], part_in.at[k, n], ex_send.at[k], ex_recv.at[k, n], tp=partner
             )
+            exch[k, n].start()
             keep_b[k, n] = both[:piece]
             if n:
                 relay(k, n - 1)
         relay(k, OUT_SPLITS - 1)
+        waits.append(bulk(part_out.at[k], ex_send.at[k], ex_recv.at[k, 0]))
+        waits.append(bulk(cross_out.at[k], cr_send.at[k], cr_recv.at[k, 0]))
 
     lse_near[...] = jnp.zeros_like(lse_near)
     cls_lse[...] = jnp.zeros_like(cls_lse)
     halo_early.wait_recv()
     near((far_same, far_other))
-    gathered(0, 1, 2, 4)
-    class_attend(2)
+    all_groups = range(group_count)
+    low_groups, high_groups = all_groups[: group_count // 2], all_groups[group_count // 2 :]
+    gathered(0, 1, 4, 5)
     scatter(6)
-    gathered(5)
+    class_attend(2, low_groups)
+    send_back(2, low_groups)
+    class_attend(2, high_groups)
+    send_back(2, high_groups)
+    send_sums(2)
+    gathered(6)
     class_attend(3)
     load_out.wait()
     combine(2)
+    send_back(3, all_groups)
+    send_sums(3)
     out_far(0)
+    gathered(2)
+    class_attend(0)
     combine(3)
     out_far(1)
+    send_back(0, all_groups)
+    send_sums(0)
+    halo_late = edge(1 - chip, 1)
+    gathered(3)
+    class_attend(1)
+    send_back(1, all_groups)
+    send_sums(1)
     first_half = head_lane < piece
     swap = [pltpu.roll(logw_far[k], piece, 1) for k in range(SPLITS)]
     logw_ref[:, pl.ds(row_of(far_same, 0, shard), shard)] = jnp.where(
@@ -640,23 +681,19 @@
     logw_ref[:, pl.ds(row_of(far_other, 0, shard), shard)] = jnp.where(
         first_half, swap[0], logw_far[1]
     )
-    gathered(3)
-    class_attend(0)
-    gathered(6)
-    class_attend(1)
     halo_late.wait_recv()
     near((tp, partner))
     combine(1)
     for n in range(OUT_SPLITS):
         own_out[n] = product(1, n)
-        own_exch[n] = launch(
-            remote(own_out.at[n], own_in.at[n], ox_send.at[n], ox_recv.at[n], tp=partner)
-        )
+        remote(own_out.at[n], own_in.at[n], ox_send.at[0], ox_recv.at[0], tp=partner).start()
+    own_total = bulk(own_in, ox_send.at[0], ox_recv.at[0])
+    waits.append(own_total)
     combine(0)
     for n in range(OUT_SPLITS):
         keep_d[n] = product(0, n).astype(f32)
+    own_total.wait_recv()
     for n in range(OUT_SPLITS):
-        own_exch[n].wait_recv()
         keep_d[n] = keep_d[n] + own_in[n].astype(f32)
     for k in range(SPLITS):
         for n in range(OUT_SPLITS):
@@ -684,7 +721,8 @@
     freq = np.tile(freq, PAIR // half)
     start = np.concatenate([np.arange(rows), np.arange(sp_size) * rows])
     angle = start[:, None] * freq[None, :]
-    table = jnp.asarray(np.stack([np.cos(angle), np.sin(angle)]).astype(np.float32))
+    cosine, sine = np.cos(angle), np.sin(angle)
+    table = jnp.asarray(np.stack([cosine, sine, cosine, sine]).astype(np.float32))
     f32, bf16 = jnp.float32, jnp.bfloat16
     V_, DMA = pltpu.VMEM, pltpu.SemaphoreType.DMA
     window = ROW_BLOCK + 2 * SIDE_SPAN
@@ -692,7 +730,7 @@
         V_((tp_size, shard, depth), bf16),
         V_((3, depth, col_count), bf16),
         V_((col_count, wide), bf16),
-        V_(table.shape, f32),
+        V_((2,) + table.shape[1:], f32),
         V_((rows, PAIR), f32),
         V_((rows, PAIR), f32),
         V_((rows, col_count), bf16),
@@ -706,9 +744,9 @@
         V_((rows, PAIR), f32),
         V_((rows, col_count), bf16),
         V_((rows, PAIR), f32),
-        V_((SEGMENTS, heads, PAIR), f32),
+        V_((SEGMENTS, sp_size, 1, PAIR), f32),
         V_((SEGMENTS, shard, col_count), bf16),
-        V_((SEGMENTS, sp_size, heads, PAIR), f32),
+        V_((SEGMENTS, sp_size, 1, PAIR), f32),
         V_((groups, shard, PAIR), f32),
         V_((shard, PAIR), f32),
         V_((SPLITS, heads, PAIR), f32),
@@ -725,13 +763,13 @@
         DMA((1,)), DMA((1,)),
         DMA((SPLITS,)), DMA((SPLITS,)),
         DMA((SPLITS,)), DMA((SPLITS,)),
-        DMA((len(UNITS), sp_size)), DMA((len(UNITS), sp_size)),
+        DMA((len(UNITS),)), DMA((len(UNITS),)),
         DMA((2,)), DMA((2,)),
-        DMA((SEGMENTS, sp_size)), DMA((SEGMENTS, sp_size)),
-        DMA((SEGMENTS, sp_size)), DMA((SEGMENTS, sp_size)),
-        DMA((SPLITS, OUT_SPLITS)), DMA((SPLITS, OUT_SPLITS)),
-        DMA((SPLITS, OUT_SPLITS)), DMA((SPLITS, OUT_SPLITS)),
-        DMA((OUT_SPLITS,)), DMA((OUT_SPLITS,)),
+        DMA((SEGMENTS,)), DMA((SEGMENTS,)),
+        DMA((SEGMENTS,)), DMA((SEGMENTS,)),
+        DMA((SPLITS,)), DMA((SPLITS, OUT_SPLITS)),
+        DMA((SPLITS,)), DMA((SPLITS, OUT_SPLITS)),
+        DMA((1,)), DMA((1,)),
     ]
     hbm = pl.BlockSpec(memory_space=pltpu.HBM)
     vmem = pl.BlockSpec(memory_space=pltpu.VMEM)
@@ -766,8 +804,8 @@
             and WIDEST_DILATION % sp_size == 0
             and tp_size == 2 * SPLITS
             and shard == ROW_BLOCK
-            and shard % (16 * sp_size) == 0
-            and args[1].shape[1] % (2 * PAIR) == 0
+            and shard == 16 * sp_size
+            and args[1].shape[1] == sp_size * HEAD_DIM
         )
         if whole_class:
             return fused(sp_size, tp_size, *args)

time: 88 us -> 80.2 us (0.911)
  Pallas kernels: 84.6 us -> 77.8 us
  local copies, waits for them, and re-layouts: 2.62 us -> 1.58 us
    pallas_call x1, Pallas kernels: 84.6 us -> 77.8 us  [fused(): pl.pallas_call(functools.partial(class_kernel, sp_size, tp_size, col_coun...]
    unnamed x4 -> x2, local copies, waits for them, and re-layouts: 2.62 us -> 1.58 us
where the time goes in v2:
time: 80.2 us; the launch traced here: 80 us
  Pallas kernels  77.8 us (97%)
  local copies, waits for them, and re-layouts  1.58 us (2%)
    pallas_call x1, Pallas kernels, fused(): pl.pallas_call(functools.partial(class_kernel, sp_size, tp_size, col_coun...  77.8 us

profile of v2, /device:TPU:0, one launch (start us, length us, event | category | flops | bytes accessed | tf_op | source)
XLA Modules:
  0.0 80.0 jit_solution(15064907062050039530)
XLA Ops:
  0.6 77.8 %dilated_layer.1 = (bf16[128,4096]{1,0:T(8,128)(2,1)S(1)}, f32[8,512]{1,0:T(8,128)S(1)}) custom-call(bf16[128,4096]{1,0:T(8,128)(2,1)} %x_hbm.1, bf16[4096,512]{1,0:T(8,128)(2,1)} %wq_hbm.1, bf16[4096,512]{1,0:T(8,128)(2,1)} %wk_hbm.1, bf16[4096,512]{1,0:T(8,128)(2,1)} %wv_hbm.1, bf16[512,4096]{1,0:T(8,128)(2,1)} %wo_hbm.1, ...), custom_call_target="tpu_custom_call" | custom-call | tf_op jit(solution)/shard_map/dilated_layer/pallas_call | solution.py:776
  78.5 1.0 %copy.10 = bf16[128,4096]{1,0:T(8,128)(2,1)} copy(bf16[128,4096]{1,0:T(8,128)(2,1)S(1)} %get-tuple-element.4) | data formatting | bytes 2097152
  79.4 0.6 copy.11

commit v3 on v2

--- a/solution.py
+++ b/solution.py
@@ -209,7 +209,7 @@
     out_ref, logw_ref,
     x_all, w_all, wo, table, cos_t, sin_t, q_c, kv_ext, pf, cls_send, cls_recv,
     bias_near, bias_class, o_near, lse_near, cls_o, cls_lse, lse_out, ret, ret_lse, ret_f, lse_f, logw_far,
-    att, part_out, part_in, cross_out, cross_in, keep_b, keep_d, own_out, own_in,
+    lead_o, lead_top, lead_total, att, part_out, part_in, cross_out, cross_in, keep_b, keep_d, own_out, own_in,
     load_sem, own_send, own_recv, far_send, far_recv, fwd_send, fwd_recv,
     a2a_send, a2a_recv, halo_send, halo_recv, back_send, back_recv, lback_send, lback_recv,
     ex_send, ex_recv, cr_send, cr_recv, ox_send, ox_recv,
@@ -438,7 +438,6 @@
     project(0, Q)
     scatter(2)
     project(1, Q)
-    scatter(3)
 
     fwd = []
     for k in range(SPLITS):
@@ -467,20 +466,36 @@
     lane_wide = lax.broadcasted_iota(jnp.int32, (ROW_BLOCK, PAIR), 1)
     scale = HEAD_DIM ** (-0.5)
 
-    def attend(query, keys, values, bias):
-        outs, sums = [], []
-        for half in range(2):
-            pick = first_head if half == 0 else jnp.logical_not(first_head)
-            q = jnp.where(pick, query.astype(f32) * scale, 0.0).astype(bf16)
-            s = lax.dot_general(q, keys, (((1,), (1,)), ((), ())), preferred_element_type=f32)
+    def pair_scores(query, keys):
+        q = query.astype(f32) * scale
+        both = jnp.concatenate(
+            [jnp.where(first_head, q, 0.0), jnp.where(first_head, 0.0, q)], axis=0
+        ).astype(bf16)
+        s = lax.dot_general(both, keys, (((1,), (1,)), ((), ())), preferred_element_type=f32)
+        return s[: query.shape[0]], s[query.shape[0] :]
+
+    def pair_product(e, values):
+        o = jnp.dot(
+            jnp.concatenate(e, axis=0).astype(bf16), values, preferred_element_type=f32
+        )
+        return o[: e[0].shape[0]], o[e[0].shape[0] :]
+
+    def soften(query, keys, bias):
+        e, tops, totals = [], [], []
+        for s in pair_scores(query, keys):
             s = s + bias
             top = jnp.max(s, axis=1, keepdims=True)
-            e = jnp.exp(s - top)
-            total = jnp.sum(e, axis=1, keepdims=True)
-            o = jnp.dot(e.astype(bf16), values, preferred_element_type=f32)
-            outs.append(o / total)
-            sums.append(top + jnp.log(total))
-        return jnp.where(first_head, outs[0], outs[1]), sums
+            part = jnp.exp(s - top)
+            e.append(part)
+            tops.append(top)
+            totals.append(jnp.sum(part, axis=1, keepdims=True))
+        return e, tops, totals
+
+    def attend(query, keys, values, bias):
+        e, tops, totals = soften(query, keys, bias)
+        o = pair_product(e, values)
+        sums = [top + jnp.log(total) for top, total in zip(tops, totals)]
+        return jnp.where(first_head, o[0] / totals[0], o[1] / totals[1]), sums
 
     def keep_sums(ref, span, g, sums):
         kept = ref[span]
@@ -513,7 +528,7 @@
     def lback_total(seg):
         return bulk(ret_lse.at[seg, pl.ds(0, sp_size - 1)], lback_send.at[seg], lback_recv.at[seg])
 
-    def class_attend(seg, groups=None):
+    def class_attend(seg):
         span = slice(seg * shard, (seg + 1) * shard)
 
         def block(g):
@@ -532,11 +547,56 @@
             block(2 * i + 1)
             return carry
 
-        if groups is None:
-            lax.fori_loop(0, group_count // 2, two, 0)
-        else:
-            for g in groups:
-                block(g)
+        lax.fori_loop(0, group_count // 2, two, 0)
+
+    lead_keys = (SEGMENTS - 1) * shard
+
+    def class_lead(seg):
+        span = slice(seg * shard, (seg + 1) * shard)
+
+        def one(g, carry):
+            c0 = pl.multiple_of(g * PAIR, PAIR)
+            e, tops, totals = soften(
+                cls_recv[span, pl.ds(c0 + Q * col_count, PAIR)],
+                cls_recv[:lead_keys, pl.ds(c0 + K * col_count, PAIR)],
+                bias_class[span, :lead_keys],
+            )
+            o = pair_product(e, cls_recv[:lead_keys, pl.ds(c0 + V * col_count, PAIR)])
+            lead_o[g] = jnp.where(first_head, o[0], o[1])
+            for half in range(2):
+                lead_top[2 * g + half] = jnp.broadcast_to(tops[half], (shard, PAIR))
+                lead_total[2 * g + half] = jnp.broadcast_to(totals[half], (shard, PAIR))
+            return carry
+
+        def two(i, carry):
+            one(2 * i, carry)
+            return one(2 * i + 1, carry)
+
+        lax.fori_loop(0, group_count // 2, two, 0)
+
+    def class_rest(seg, groups):
+        span = slice(seg * shard, (seg + 1) * shard)
+        for g in groups:
+            cols = [slice(n * col_count + g * PAIR, n * col_count + (g + 1) * PAIR) for n in (K, V, Q)]
+            parts = pair_scores(cls_recv[span, cols[Q]], cls_recv[lead_keys:, cols[K]])
+            e, sums, decays, totals = [], [], [], []
+            for half, s in enumerate(parts):
+                s = s + bias_class[span, lead_keys:]
+                old = lead_top[2 * g + half]
+                top = jnp.maximum(old, jnp.max(s, axis=1, keepdims=True))
+                part = jnp.exp(s - top)
+                decay = jnp.exp(old - top)
+                total = lead_total[2 * g + half] * decay + jnp.sum(part, axis=1, keepdims=True)
+                e.append(part)
+                decays.append(decay)
+                totals.append(total)
+                sums.append(top + jnp.log(total))
+            o = pair_product(e, cls_recv[lead_keys:, cols[V]])
+            o = jnp.where(first_head, o[0], o[1])
+            decay = jnp.where(first_head, decays[0], decays[1])
+            total = jnp.where(first_head, totals[0], totals[1])
+            cls_o[span, g * PAIR : (g + 1) * PAIR] = ((lead_o[g] * decay + o) / total).astype(bf16)
+            keep_sums(cls_lse, span, g, sums)
 
     def send_back(seg, groups):
         cols = slice(groups[0] * PAIR, (groups[-1] + 1) * PAIR)
@@ -648,31 +708,38 @@
     near((far_same, far_other))
     all_groups = range(group_count)
     low_groups, high_groups = all_groups[: group_count // 2], all_groups[group_count // 2 :]
-    gathered(0, 1, 4, 5)
-    scatter(6)
-    class_attend(2, low_groups)
+    gathered(0, 1, 4)
+    class_lead(2)
+    all_groups = range(group_count)
+    low_groups, high_groups = all_groups[: group_count // 2], all_groups[group_count // 2 :]
+    gathered(5)
+    class_rest(2, low_groups)
     send_back(2, low_groups)
-    class_attend(2, high_groups)
+    class_rest(2, high_groups)
     send_back(2, high_groups)
     send_sums(2)
+    gathered(2)
+    class_attend(0)
+    scatter(6)
+    load_out.wait()
+    combine(2)
+    scatter(3)
+    halo_late = edge(1 - chip, 1)
+    out_far(0)
     gathered(6)
     class_attend(3)
-    load_out.wait()
-    combine(2)
     send_back(3, all_groups)
     send_sums(3)
-    out_far(0)
-    gathered(2)
-    class_attend(0)
+    gathered(3)
+    class_attend(1)
+    halo_late.wait_recv()
+    near((tp, partner))
+    send_back(1, all_groups)
+    send_sums(1)
     combine(3)
-    out_far(1)
     send_back(0, all_groups)
     send_sums(0)
-    halo_late = edge(1 - chip, 1)
-    gathered(3)
-    class_attend(1)
-    send_back(1, all_groups)
-    send_sums(1)
+    out_far(1)
     first_half = head_lane < piece
     swap = [pltpu.roll(logw_far[k], piece, 1) for k in range(SPLITS)]
     logw_ref[:, pl.ds(row_of(far_same, 0, shard), shard)] = jnp.where(
@@ -681,8 +748,6 @@
     logw_ref[:, pl.ds(row_of(far_other, 0, shard), shard)] = jnp.where(
         first_half, swap[0], logw_far[1]
     )
-    halo_late.wait_recv()
-    near((tp, partner))
     combine(1)
     for n in range(OUT_SPLITS):
         own_out[n] = product(1, n)
@@ -750,6 +815,9 @@
         V_((groups, shard, PAIR), f32),
         V_((shard, PAIR), f32),
         V_((SPLITS, heads, PAIR), f32),
+        V_((groups, shard, PAIR), f32),
+        V_((heads, shard, PAIR), f32),
+        V_((heads, shard, PAIR), f32),
         V_((SEGMENTS, shard, col_count), bf16),
         V_((SPLITS, OUT_SPLITS, piece, width), bf16),
         V_((SPLITS, OUT_SPLITS, piece, width), bf16),

time: 80.2 us -> 77.4 us (0.965)
  Pallas kernels: 77.8 us -> 75.1 us
    pallas_call x1, Pallas kernels: 77.8 us -> 75.1 us  [fused(): pl.pallas_call(functools.partial(class_kernel, sp_size, tp_size, col_coun...]
where the time goes in v3:
time: 77.4 us; the launch traced here: 77.3 us
  Pallas kernels  75.1 us (97%)
  local copies, waits for them, and re-layouts  1.58 us (2%)
    pallas_call x1, Pallas kernels, fused(): pl.pallas_call(functools.partial(class_kernel, sp_size, tp_size, col_coun...  75.1 us
    unnamed x2, local copies, waits for them, and re-layouts  1.58 us

profile of v3, /device:TPU:0, one launch (start us, length us, event | category | flops | bytes accessed | tf_op | source)
XLA Modules:
  0.0 77.3 jit_solution(6039278167066255798)
XLA Ops:
  0.6 75.1 %dilated_layer.1 = (bf16[128,4096]{1,0:T(8,128)(2,1)S(1)}, f32[8,512]{1,0:T(8,128)S(1)}) custom-call(bf16[128,4096]{1,0:T(8,128)(2,1)} %x_hbm.1, bf16[4096,512]{1,0:T(8,128)(2,1)} %wq_hbm.1, bf16[4096,512]{1,0:T(8,128)(2,1)} %wk_hbm.1, bf16[4096,512]{1,0:T(8,128)(2,1)} %wv_hbm.1, bf16[512,4096]{1,0:T(8,128)(2,1)} %wo_hbm.1, ...), custom_call_target="tpu_custom_call" | custom-call | tf_op jit(solution)/shard_map/dilated_layer/pallas_call | solution.py:844
  75.7 1.0 %copy.10 = bf16[128,4096]{1,0:T(8,128)(2,1)} copy(bf16[128,4096]{1,0:T(8,128)(2,1)S(1)} %get-tuple-element.4) | data formatting | bytes 2097152
  76.7 0.6 copy.11

commit v4 on v3

--- a/solution.py
+++ b/solution.py
@@ -435,9 +435,9 @@
     scatter(1)
     halo_early = edge(chip, 0)
     load_w[Q].wait()
+    project(1, Q)
+    scatter(3)
     project(0, Q)
-    scatter(2)
-    project(1, Q)
 
     fwd = []
     for k in range(SPLITS):
@@ -528,7 +528,7 @@
     def lback_total(seg):
         return bulk(ret_lse.at[seg, pl.ds(0, sp_size - 1)], lback_send.at[seg], lback_recv.at[seg])
 
-    def class_attend(seg):
+    def class_attend(seg, groups=None):
         span = slice(seg * shard, (seg + 1) * shard)
 
         def block(g):
@@ -547,7 +547,11 @@
             block(2 * i + 1)
             return carry
 
-        lax.fori_loop(0, group_count // 2, two, 0)
+        if groups is None:
+            lax.fori_loop(0, group_count // 2, two, 0)
+        else:
+            for g in groups:
+                block(g)
 
     lead_keys = (SEGMENTS - 1) * shard
 
@@ -687,8 +691,8 @@
         )
         cross[k, n].start()
 
-    def out_far(k):
-        for n in range(OUT_SPLITS):
+    def out_far(k, chunks):
+        for n in chunks:
             both = product(2 + k, n)
             part_out[k, n] = both[piece:]
             exch[k, n] = remote(
@@ -696,11 +700,12 @@
             )
             exch[k, n].start()
             keep_b[k, n] = both[:piece]
-            if n:
+            if n != chunks[0]:
                 relay(k, n - 1)
-        relay(k, OUT_SPLITS - 1)
-        waits.append(bulk(part_out.at[k], ex_send.at[k], ex_recv.at[k, 0]))
-        waits.append(bulk(cross_out.at[k], cr_send.at[k], cr_recv.at[k, 0]))
+        relay(k, chunks[-1])
+        if chunks[-1] == OUT_SPLITS - 1:
+            waits.append(bulk(part_out.at[k], ex_send.at[k], ex_recv.at[k, 0]))
+            waits.append(bulk(cross_out.at[k], cr_send.at[k], cr_recv.at[k, 0]))
 
     lse_near[...] = jnp.zeros_like(lse_near)
     cls_lse[...] = jnp.zeros_like(cls_lse)
@@ -718,28 +723,32 @@
     class_rest(2, high_groups)
     send_back(2, high_groups)
     send_sums(2)
-    gathered(2)
-    class_attend(0)
+    gathered(3)
+    class_attend(1)
     scatter(6)
     load_out.wait()
     combine(2)
-    scatter(3)
     halo_late = edge(1 - chip, 1)
-    out_far(0)
+    all_chunks = range(OUT_SPLITS)
+    out_far(0, all_chunks[: OUT_SPLITS // 2])
     gathered(6)
-    class_attend(3)
-    send_back(3, all_groups)
+    class_attend(3, low_groups)
+    send_back(3, low_groups)
+    class_attend(3, high_groups)
+    send_back(3, high_groups)
     send_sums(3)
-    gathered(3)
-    class_attend(1)
+    out_far(0, all_chunks[OUT_SPLITS // 2 :])
+    scatter(2)
     halo_late.wait_recv()
     near((tp, partner))
+    combine(3)
     send_back(1, all_groups)
     send_sums(1)
-    combine(3)
+    out_far(1, all_chunks)
+    gathered(2)
+    class_attend(0)
     send_back(0, all_groups)
     send_sums(0)
-    out_far(1)
     first_half = head_lane < piece
     swap = [pltpu.roll(logw_far[k], piece, 1) for k in range(SPLITS)]
     logw_ref[:, pl.ds(row_of(far_same, 0, shard), shard)] = jnp.where(

time: 77.4 us -> 76.3 us (0.986)
  Pallas kernels: 75.1 us -> 73.9 us
    pallas_call x1, Pallas kernels: 75.1 us -> 73.9 us  [fused(): pl.pallas_call(functools.partial(class_kernel, sp_size, tp_size, col_coun...]
where the time goes in v4:
time: 76.3 us; the launch traced here: 76.2 us
  Pallas kernels  73.9 us (97%)
  local copies, waits for them, and re-layouts  1.58 us (2%)
    pallas_call x1, Pallas kernels, fused(): pl.pallas_call(functools.partial(class_kernel, sp_size, tp_size, col_coun...  73.9 us
    unnamed x2, local copies, waits for them, and re-layouts  1.58 us

profile of v4, /device:TPU:0, one launch (start us, length us, event | category | flops | bytes accessed | tf_op | source)
XLA Modules:
  0.0 76.2 jit_solution(1182425415815581984)
XLA Ops:
  0.6 73.9 %dilated_layer.1 = (bf16[128,4096]{1,0:T(8,128)(2,1)S(1)}, f32[8,512]{1,0:T(8,128)S(1)}) custom-call(bf16[128,4096]{1,0:T(8,128)(2,1)} %x_hbm.1, bf16[4096,512]{1,0:T(8,128)(2,1)} %wq_hbm.1, bf16[4096,512]{1,0:T(8,128)(2,1)} %wk_hbm.1, bf16[4096,512]{1,0:T(8,128)(2,1)} %wv_hbm.1, bf16[512,4096]{1,0:T(8,128)(2,1)} %wo_hbm.1, ...), custom_call_target="tpu_custom_call" | custom-call | tf_op jit(solution)/shard_map/dilated_layer/pallas_call | solution.py:853
  74.6 1.0 %copy.10 = bf16[128,4096]{1,0:T(8,128)(2,1)} copy(bf16[128,4096]{1,0:T(8,128)(2,1)S(1)} %get-tuple-element.4) | data formatting | bytes 2097152
  75.6 0.6 copy.11
